TPU v7x, 256 devices: a whole 4x4x8 slice. The times are simulated.
256 devices in a mesh: ep: 128 (over z, y, x), tp: 2 (over core).
Axes of the slice: x: 4, y: 4, z: 8, core: 2. Of those that a mesh axis runs over, the one named last changes fastest.
Arguments:
- tokens: bfloat16 [3072, 2048], P('ep'), may hold values from -40 to 40
- old_state: float32 [3072, 16, 4096], P('ep', 'tp'), may hold values from -6 to 6
- w_query: bfloat16 [2048, 1024], P(None, 'tp'), may hold values from -0.125 to 0.125
- w_forget: bfloat16 [2048, 1024], P(None, 'tp'), may hold values from -0.125 to 0.125
- w_value: bfloat16 [2048, 1024], P(None, 'tp'), may hold values from -0.125 to 0.125
- w_gate: bfloat16 [2048, 1024], P(None, 'tp'), may hold values from -0.125 to 0.125
- lower_bound: float32 [1024], P('tp'), may hold values from 0.05 to 0.9
- head_gain: float32 [64], replicated, may hold values from 0.1 to 1.9
- w_out: bfloat16 [1024, 2048], P('tp'), may hold values from -0.1875 to 0.1875
- mix_gain: float32 [2048], replicated, may hold values from 0.1 to 1.9
- expert_gate: bfloat16 [128, 2048, 512], P('ep', None, 'tp'), may hold values from -0.125 to 0.125
- expert_up: bfloat16 [128, 2048, 512], P('ep', None, 'tp'), may hold values from -0.125 to 0.125
- expert_down: bfloat16 [128, 512, 2048], P('ep', 'tp'), may hold values from -0.25 to 0.25
- expert_ids: int32 [3072, 2], P('ep'), may hold values from 0 to 127, as said below
- route_weight: float32 [3072, 2], P('ep'), may hold values from 0.1 to 1
- moe_gain: float32 [2048], replicated, may hold values from 0.1 to 1.9
Outputs:
- next_tokens: bfloat16 [3072, 2048], P('ep', 'tp')
- new_state: float32 [3072, 16, 4096], P('ep', 'tp')
Inputs may be any that keep to these rules, and one draw needn't show every extreme that they name: `expert_ids`: each row names two different experts of one group of 4 consecutive experts. In each aligned block of 24 rows no expert is named by more than 2 rows, and one expert, the same in every block, is named by exactly 2 rows of every block.
All inputs are finite; a program needn't handle non-finite values.
Results may differ from a plain program's by a relative error of at most 0.011.
Values may be sent and summed in bfloat16 or wider, within the bound.
A program may use at most 128 MiB of HBM per device.

v0:
```python
import jax
import jax.numpy as jnp
from jax import lax
from jax.sharding import PartitionSpec as P


def sent_to_all(array, axis):
    copies = jnp.broadcast_to(array, (lax.axis_size(axis), *array.shape))
    return lax.all_to_all(copies, axis, split_axis=0, concat_axis=0, tiled=True)


def of_everyone(array, axis):
    everything = sent_to_all(array, axis)
    return jnp.sum(everything.astype(jnp.float32), axis=0)


def cut_along(array, dim, peers):
    shape = array.shape
    blocks = array.reshape(*shape[:dim], peers, shape[dim] // peers, *shape[dim + 1 :])
    return jnp.moveaxis(blocks, dim, 0)


def sent_and_summed(array, axis, dim):
    blocks = cut_along(array, dim, lax.axis_size(axis))
    arrived = lax.all_to_all(blocks, axis, split_axis=0, concat_axis=0, tiled=True)
    return arrived.astype(jnp.float32).sum(axis=0)


def in_order(blocks, dim):
    blocks = jnp.moveaxis(blocks, 0, dim)
    shape = blocks.shape
    return blocks.reshape(*shape[:dim], shape[dim] * shape[dim + 1], *shape[dim + 2 :])


def collect(array, axis, dim):
    blocks = sent_to_all(array, axis)
    return in_order(blocks, dim)


def layer_normed(values, gain):
    center = jnp.mean(values, -1, keepdims=True)
    centered = values - center
    variance = jnp.mean(centered * centered, -1, keepdims=True)
    return centered * lax.rsqrt(variance + 1e-05) * gain


def rounded(values):
    return lax.optimization_barrier(values.astype(jnp.bfloat16)).astype(jnp.float32)


def slot_table(ids_block, expert_count, capacity):
    flat_ids = ids_block.reshape(-1)
    onehot = (flat_ids[:, None] == jnp.arange(expert_count, dtype=jnp.int32)[None, :]).astype(
        jnp.int32
    )
    before = jnp.cumsum(onehot, 0) - onehot
    rank = jnp.sum(before * onehot, 1)
    return flat_ids * capacity + rank


def per_device(
    tokens,
    old_state,
    w_query,
    w_forget,
    w_value,
    w_gate,
    lower_bound,
    head_gain,
    w_out,
    mix_gain,
    expert_gate,
    expert_up,
    expert_down,
    expert_ids,
    route_weight,
    moe_gain,
):
    row_count, model_width = tokens.shape
    heads_here = old_state.shape[1]
    head_dim = head_gain.shape[0]
    head_cols = w_query.shape[1]
    q_lin = jnp.dot(tokens, w_query, preferred_element_type=jnp.float32)
    f_lin = jnp.dot(tokens, w_forget, preferred_element_type=jnp.float32)
    v_lin = jnp.dot(tokens, w_value, preferred_element_type=jnp.float32)
    g_lin = jnp.dot(tokens, w_gate, preferred_element_type=jnp.float32)
    act_query = jax.nn.silu(q_lin).reshape(row_count, heads_here, head_dim)
    bound = lower_bound.reshape(heads_here, head_dim)
    forget = bound + (1.0 - bound) * jax.nn.sigmoid(f_lin.reshape(row_count, heads_here, head_dim))
    previous = old_state.reshape(row_count, heads_here, head_dim, head_dim)
    new_state = forget[..., None] * previous + (1.0 - forget)[..., None] * v_lin.reshape(
        row_count, heads_here, 1, head_dim
    )
    readout = jnp.einsum("shi,shij->shj", act_query, new_state)
    normed = readout * lax.rsqrt(jnp.mean(readout * readout, -1, keepdims=True) + 1e-06) * head_gain
    mixer_out = (
        (normed * jax.nn.silu(g_lin.reshape(row_count, heads_here, head_dim)))
        .reshape(row_count, head_cols)
        .astype(jnp.bfloat16)
    )
    own_part = rounded(jnp.dot(mixer_out, w_out, preferred_element_type=jnp.float32))
    mixed = of_everyone(own_part.astype(jnp.bfloat16), "tp").astype(jnp.float32)
    after_mixer = layer_normed(tokens.astype(jnp.float32) + mixed, mix_gain).astype(jnp.bfloat16)
    expert_count = lax.axis_size("ep")
    core_count = lax.axis_size("tp")
    top_count = expert_ids.shape[1]
    capacity = max(2, 2 * top_count * row_count // expert_count)
    slot_ids = slot_table(expert_ids, expert_count, capacity)
    choose = (
        slot_ids[None, :] == jnp.arange(expert_count * capacity, dtype=jnp.int32)[:, None]
    ).astype(jnp.bfloat16)
    choose = choose.reshape(expert_count * capacity, row_count, top_count).sum(-1)
    outgoing = jnp.dot(choose, after_mixer, preferred_element_type=jnp.float32).astype(jnp.bfloat16)
    outgoing = outgoing.reshape(expert_count, capacity, model_width)
    arrived = lax.all_to_all(outgoing, "ep", split_axis=0, concat_axis=0, tiled=True)
    sources = arrived.shape[0]
    slots_now = arrived.shape[1]
    rows_in = arrived.reshape(sources * slots_now, model_width)
    gate_act = jnp.dot(rows_in, expert_gate[0], preferred_element_type=jnp.float32)
    up_act = jnp.dot(rows_in, expert_up[0], preferred_element_type=jnp.float32)
    hidden = (jax.nn.silu(gate_act) * up_act).astype(jnp.bfloat16)
    partial_rows = rounded(jnp.dot(hidden, expert_down[0], preferred_element_type=jnp.float32))
    summed_rows = sent_and_summed(partial_rows.astype(jnp.bfloat16), "tp", 1)
    results = summed_rows.astype(jnp.bfloat16).reshape(sources, slots_now, summed_rows.shape[1])
    back_half = lax.all_to_all(results, "ep", split_axis=0, concat_axis=0, tiled=True)
    returned = collect(back_half, "tp", 2)
    flat_back = returned.reshape(expert_count * capacity, model_width)
    picked = (
        jnp.take(flat_back, slot_ids, axis=0)
        .reshape(row_count, top_count, model_width)
        .astype(jnp.float32)
    )
    moe_sum = jnp.sum(picked * route_weight[..., None], 1)
    full_rows = layer_normed(after_mixer.astype(jnp.float32) + moe_sum, moe_gain).astype(
        jnp.bfloat16
    )
    half_width = model_width // core_count
    next_tokens = lax.dynamic_slice_in_dim(
        full_rows, lax.axis_index("tp") * half_width, half_width, 1
    )
    return (next_tokens, new_state.reshape(row_count, heads_here, head_dim * head_dim))


def solution(mesh):
    in_specs = (
        P("ep", None),
        P("ep", "tp", None),
        P(None, "tp"),
        P(None, "tp"),
        P(None, "tp"),
        P(None, "tp"),
        P("tp"),
        P(),
        P("tp", None),
        P(),
        P("ep", None, "tp"),
        P("ep", None, "tp"),
        P("ep", "tp", None),
        P("ep", None),
        P("ep", None),
        P(),
    )
    out_specs = (P("ep", "tp"), P("ep", "tp", None))
    return jax.shard_map(
        per_device, mesh=mesh, in_specs=in_specs, out_specs=out_specs, check_vma=False
    )
```

profile of v0, /device:TPU:1, one launch (start us, length us, event | category | flops | bytes accessed | tf_op | source)
XLA Modules:
  0.0 129.8 jit_solution(8123525983972221120)
XLA Ops:
  0.6 0.0 copy-start
  0.6 0.9 add.124
  1.6 2.1 %fusion.7 = f32[24,512]{1,0:T(8,128)S(1)} fusion(bf16[24,2048]{1,0:T(8,128)(2,1)} %param.16, bf16[2048,512]{1,0:T(8,128)(2,1)} %param.19), kind=kOutput, calls=%fused_computation.15 | convolution fusion | flops 50368512 | bytes 2244608 | tf_op jit(solution)/shard_map/dot_general | solution.py:84
  3.6 0.1 div.45
  3.7 2.0 %fusion.32 = f32[24,512]{1,0:T(8,128)S(1)} fusion(bf16[24,2048]{1,0:T(8,128)(2,1)} %param.16, bf16[2048,512]{1,0:T(8,128)(2,1)} %param.20), kind=kOutput, calls=%fused_computation.67 | convolution fusion | flops 50331648 | bytes 2244608 | tf_op jit(solution)/shard_map/dot_general | solution.py:85
  5.7 0.1 mul.165
  5.8 6.1 %reshape.162 = f32[24,8,64,64]{3,2,1,0:T(8,128)} reshape(f32[24,8,4096]{2,1,0:T(8,128)} %param.17) | data formatting | bytes 6291456 | tf_op jit(solution)/shard_map/reshape | solution.py:90
  12.0 2.0 %divide_multiply_fusion = f32[24,512]{1,0:T(8,128)S(1)} fusion(bf16[24,2048]{1,0:T(8,128)(2,1)S(1)} %copy-done.1, bf16[2048,512]{1,0:T(8,128)(2,1)} %param.18), kind=kOutput, calls=%fused_computation.46 | convolution fusion | flops 50380800 | bytes 2244608 | tf_op jit(solution)/shard_map/dot_general | solution.py:83
  14.0 0.1 reshape.177
  14.1 0.0 copy-start.7
  14.1 6.0 %fusion = f32[24,8,1,64]{3,2,1,0:T(1,128)S(1)} fusion(f32[24,8,64,1]{2,3,1,0:T(1,128)S(1)} %bitcast.56, f32[24,8,64,64]{3,2,1,0:T(8,128)} %reshape.162, f32[24,8,64]{2,1,0:T(8,128)S(1)} %get-tuple-element.7, f32[24,8,64]{2,1,0:T(8,128)S(1)} %mul.165, f32[24,8,64]{2,1,0:T(8,128)S(1)} %get-tuple-element.6), kind=kOutput, calls=%fused_computation.1 | convolution fusion | flops 3932160 | bytes 3391488 | tf_op jit(solution)/shard_map/shi,shij->shj/dot_general | solution.py:94
  20.1 0.1 multiply_reduce_fusion.3
  20.3 0.0 copy-start.3
  20.3 0.4 fusion.33
  20.7 0.1 reshape.163
  20.8 0.1 multiply_convert_fusion.1
  20.9 0.1 convert_element_type.53
  21.0 0.4 convolution_convert_fusion.2
  21.4 6.7 %all_to_all.25 = bf16[2,24,2048]{2,1,0:T(8,128)(2,1)S(1)} all-to-all(bf16[2,24,2048]{2,1,0:T(8,128)(2,1)S(1)} %broadcast_in_dim.11), channel_id=1, replica_groups=mesh['ep'=128,'tp'=2] {'tp'}, dimensions={0} | all-to-all | bytes 393216 | tf_op jit(solution)/shard_map/all_to_all | solution.py:9
  28.2 0.1 fusion.23
  28.3 0.2 multiply_reduce_fusion.2
  28.6 0.1 copy.35
  28.6 0.1 reshape.164
  28.7 0.1 fusion.26
  28.8 0.1 reduce_window_sum.11
  28.9 0.2 select_reduce_fusion
  29.1 0.1 reduce_sum.105
  29.2 0.1 copy.36
  29.3 0.5 compare_and_fusion
  29.8 0.1 fusion.25
  29.9 0.1 multiply_convert_fusion
  30.0 0.5 convolution_convert_fusion
  30.5 1.5 %reshape.165 = bf16[128,2,2048]{2,1,0:T(2,128)(2,1)} reshape(bf16[256,2048]{1,0:T(8,128)(2,1)S(1)} %convolution_convert_fusion) | data formatting | bytes 2097152 | tf_op jit(solution)/shard_map/reshape | solution.py:114
  31.9 13.8 %all-to-all-start.1 = ((bf16[128,2,2048]{2,1,0:T(2,128)(2,1)}), bf16[128,2,2048]{2,1,0:T(2,128)(2,1)S(1)}, u32[]{:S(2)}, u32[]{:S(2)}) async-start(bf16[128,2,2048]{2,1,0:T(2,128)(2,1)} %reshape.165), calls=%async_computation.1 | async-start | bytes 2097152 | tf_op jit(solution)/shard_map/all_to_all | solution.py:115
  45.8 0.1 copy.40
  45.9 0.6 mul.185
  46.4 0.7 copy.37
  47.2 0.8 copy.41
  47.9 3.8 %broadcast_multiply_fusion = f32[24,8,64,64]{3,2,1,0:T(8,128)} fusion(f32[24,8,64]{2,1,0:T(8,128)S(1)} %mul.165, f32[24,8,64]{2,1,0:T(8,128)S(1)} %get-tuple-element.6), kind=kLoop, calls=%fused_computation.5 | loop fusion | flops 786432 | bytes 3244032 | tf_op jit(solution)/shard_map/mul | solution.py:91
  51.7 5.8 %mul.196 = f32[24,8,4096]{2,1,0:T(8,128)} reshape(f32[24,8,64,64]{3,2,1,0:T(8,128)} %broadcast_multiply_fusion) | data formatting | bytes 6291456 | tf_op jit(solution)/shard_map/mul | solution.py:91
  57.6 3.8 %mul.162 = f32[24,8,64,64]{3,2,1,0:T(8,128)} broadcast(f32[24,8,64]{2,1,0:T(8,128)S(1)} %get-tuple-element.7), dimensions={0,1,2} | broadcast | bytes 3194880 | tf_op jit(solution)/shard_map/mul | solution.py:91
  61.4 5.9 %mul.194 = f32[24,8,4096]{2,1,0:T(8,128)} reshape(f32[24,8,64,64]{3,2,1,0:T(8,128)} %mul.162) | data formatting | bytes 6291456 | tf_op jit(solution)/shard_map/mul | solution.py:91
  67.3 7.6 %all-to-all-done.1 = bf16[128,2,2048]{2,1,0:T(2,128)(2,1)S(1)} async-done(((bf16[128,2,2048]{2,1,0:T(2,128)(2,1)}), bf16[128,2,2048]{2,1,0:T(2,128)(2,1)S(1)}, u32[]{:S(2)}, u32[]{:S(2)}) %all-to-all-start.1) | async-done | bytes 1048608 | tf_op jit(solution)/shard_map/all_to_all | solution.py:115
  74.9 1.2 reshape.166
  76.1 2.0 %fusion.11 = f32[256,256]{1,0:T(8,128)S(1)} fusion(bf16[256,2048]{1,0:T(8,128)(2,1)} %reshape.166, bf16[1,2048,256]{2,1,0:T(8,128)(2,1)} %param.26), kind=kOutput, calls=%fused_computation.19 | convolution fusion | flops 268435456 | bytes 2359296 | tf_op jit(solution)/shard_map/dot_general | solution.py:119
  78.1 3.1 %convolution_convert_fusion.1 = bf16[256,2048]{1,0:T(8,128)(2,1)S(1)} fusion(bf16[256,2048]{1,0:T(8,128)(2,1)} %reshape.166, bf16[1,256,2048]{2,1,0:T(8,128)(2,1)} %param.28, bf16[1,2048,256]{2,1,0:T(8,128)(2,1)} %param.27, f32[256,256]{1,0:T(8,128)S(1)} %fusion.11), kind=kOutput, calls=%fused_computation.8 | convolution fusion | flops 537788416 | bytes 4456448 | tf_op jit(solution)/shard_map/dot_general | solution.py:122
  81.2 0.1 copy.47
  81.3 7.3 %all_to_all.26 = bf16[2,256,1024]{2,1,0:T(8,128)(2,1)S(1)} all-to-all(bf16[2,256,1024]{2,1,0:T(8,128)(2,1)S(1)} %bitcast.50), channel_id=1, replica_groups=mesh['ep'=128,'tp'=2] {'tp'}, dimensions={0} | all-to-all | bytes 2097152 | tf_op jit(solution)/shard_map/all_to_all | solution.py:25
  88.6 1.2 reduce_sum.107
  89.7 2.0 %reshape.168 = bf16[128,2,1024]{2,1,0:T(2,128)(2,1)} reshape(bf16[256,1024]{1,0:T(8,128)(2,1)} %reduce_sum.107) | data formatting | bytes 1048576 | tf_op jit(solution)/shard_map/reshape | solution.py:124
  91.8 6.4 %all-to-all-start.3 = ((bf16[128,2,1024]{2,1,0:T(2,128)(2,1)}), bf16[128,2,1024]{2,1,0:T(2,128)(2,1)S(1)}, u32[]{:S(2)}, u32[]{:S(2)}) async-start(bf16[128,2,1024]{2,1,0:T(2,128)(2,1)} %reshape.168), calls=%async_computation.3 | async-start | bytes 1048576 | tf_op jit(solution)/shard_map/all_to_all | solution.py:125
  98.1 6.2 %multiply_add_fusion = f32[24,8,4096]{2,1,0:T(8,128)} fusion(f32[24,8,4096]{2,1,0:T(8,128)} %mul.196, f32[24,8,4096]{2,1,0:T(8,128)} %mul.194, f32[24,8,4096]{2,1,0:T(8,128)} %param.17), kind=kLoop, calls=%fused_computation.4 | loop fusion | flops 1572864 | bytes 12582912 | tf_op jit(solution)/shard_map/add | solution.py:91
  104.3 13.0 %all-to-all-done.3 = bf16[128,2,1024]{2,1,0:T(2,128)(2,1)S(1)} async-done(((bf16[128,2,1024]{2,1,0:T(2,128)(2,1)}), bf16[128,2,1024]{2,1,0:T(2,128)(2,1)S(1)}, u32[]{:S(2)}, u32[]{:S(2)}) %all-to-all-start.3) | async-done | bytes 524320 | tf_op jit(solution)/shard_map/all_to_all | solution.py:125
  117.3 0.5 broadcast_in_dim.13
  117.8 6.7 %all_to_all.27 = bf16[2,128,2,1024]{3,2,1,0:T(2,128)(2,1)S(1)} all-to-all(bf16[2,128,2,1024]{3,2,1,0:T(2,128)(2,1)S(1)} %broadcast_in_dim.13), channel_id=1, replica_groups=mesh['ep'=128,'tp'=2] {'tp'}, dimensions={0} | all-to-all | bytes 2097152 | tf_op jit(solution)/shard_map/all_to_all | solution.py:9
  124.5 1.6 %copy.39 = bf16[128,2,2,1024]{3,2,1,0:T(2,128)(2,1)S(1)} copy(bf16[128,2,2,1024]{3,1,0,2:T(2,128)(2,1)S(1)} %bitcast.51) | data formatting | bytes 2097152 | tf_op jit(solution)/shard_map/transpose | solution.py:30
  126.1 0.0 dynamic-slice-start
  126.2 0.3 copy.45
  126.4 0.7 gather_fusion
  127.1 0.1 gather.7
  127.3 1.4 %multiply_reduce_fusion = f32[24,2048]{1,0:T(8,128)S(1)} fusion(bf16[24,2,2048]{2,1,0:T(2,128)(2,1)S(1)} %gather.7, pred[24,2]{1,0:T(8,128)(4,1)S(1)} %copy.37, f32[24,2]{1,0:T(8,128)S(1)} %copy.41), kind=kLoop, calls=%fused_computation.21 | loop fusion | flops 344064 | bytes 393456 | tf_op jit(solution)/shard_map/reduce_sum | solution.py:133
  128.7 0.1 fusion.19
  128.8 0.2 multiply_reduce_fusion.1
  129.1 0.7 fusion.22
  (28 shorter events, 0.2 us)
Async XLA Ops:
  0.6 20.4 %copy-start = (bf16[512,2048]{1,0:T(8,128)(2,1)S(1)}, bf16[512,2048]{1,0:T(8,128)(2,1)}, u32[]{:S(2)}) copy-start(bf16[512,2048]{1,0:T(8,128)(2,1)} %param.24) | copy-start | bytes 6291460
  5.8 6.1 %copy-start.1 = (bf16[24,2048]{1,0:T(8,128)(2,1)S(1)}, bf16[24,2048]{1,0:T(8,128)(2,1)}, u32[]{:S(2)}) copy-start(bf16[24,2048]{1,0:T(8,128)(2,1)} %param.16) | copy-start | bytes 294916
  14.1 6.2 %copy-start.2 = (bf16[2048,512]{1,0:T(8,128)(2,1)S(1)}, bf16[2048,512]{1,0:T(8,128)(2,1)}, u32[]{:S(2)}) copy-start(bf16[2048,512]{1,0:T(8,128)(2,1)} %param.21) | copy-start | bytes 6291460
  14.1 6.7 %copy-start.7 = (f32[64]{0:T(128)S(1)}, f32[64]{0:T(128)}, u32[]{:S(2)}) copy-start(f32[64]{0:T(128)} %param.23) | copy-start | bytes 772
  20.3 8.3 %copy-start.3 = (s32[24,2]{0,1:T(2,128)S(1)}, s32[24,2]{0,1:T(2,128)}, u32[]{:S(2)}) copy-start(s32[24,2]{0,1:T(2,128)} %param.29) | copy-start | bytes 580
  20.3 9.6 %copy-start.4 = (f32[2048]{0:T(1024)S(1)}, f32[2048]{0:T(1024)}, u32[]{:S(2)}) copy-start(f32[2048]{0:T(1024)} %param.25) | copy-start | bytes 24580
  29.1 0.8 copy-start.5
  31.9 43.0 %all-to-all-start.1 = ((bf16[128,2,2048]{2,1,0:T(2,128)(2,1)}), bf16[128,2,2048]{2,1,0:T(2,128)(2,1)S(1)}, u32[]{:S(2)}, u32[]{:S(2)}) async-start(bf16[128,2,2048]{2,1,0:T(2,128)(2,1)} %reshape.165), calls=%async_computation.1 | async-start | bytes 2097152 | tf_op jit(solution)/shard_map/all_to_all | solution.py:115
  61.4 5.9 %copy-start.6 = (s32[48]{0:T(128)S(1)}, s32[48]{0:T(128)}, u32[]{:S(2)}) copy-start(s32[48]{0:T(128)} %copy-done.5) | copy-start | bytes 580
  61.4 5.9 %copy-start.8 = (s32[48,1]{0,1:T(1,128)S(1)}, s32[48,1]{0,1:T(1,128)}, u32[]{:S(2)}) copy-start(s32[48,1]{0,1:T(1,128)} %mul.185) | copy-start | bytes 580
  91.8 25.5 %all-to-all-start.3 = ((bf16[128,2,1024]{2,1,0:T(2,128)(2,1)}), bf16[128,2,1024]{2,1,0:T(2,128)(2,1)S(1)}, u32[]{:S(2)}, u32[]{:S(2)}) async-start(bf16[128,2,1024]{2,1,0:T(2,128)(2,1)} %reshape.168), calls=%async_computation.3 | async-start | bytes 1048576 | tf_op jit(solution)/shard_map/all_to_all | solution.py:125
  126.1 2.9 %dynamic-slice-start = ((f32[2048]{0:T(1024)}, s32[]{:T(128)}), f32[1024]{0:T(1024)S(1)}, s32[]{:S(2)}) async-start(f32[2048]{0:T(1024)} %param.31, s32[]{:T(128)} %select_n.28), calls=%async_computation.5 | async-start | bytes 8704 | tf_op jit(solution)/shard_map/dynamic_slice | solution.py:138
where the time goes:
time: 131 us; the launch traced here: 130 us
  local copies, waits for them, and re-layouts  33.7 us (26%)
  blocking collectives  20.7 us (16%)
  waiting for transfers between devices  20.6 us (16%)
  starting transfers between devices  20.2 us (15%)
  matrix products  18.5 us (14%)
  other arithmetic  15.2 us (12%)
    all_to_all x1, starting transfers between devices, per_device(): lax.all_to_all(outgoing, 'ep', split_axis=0, concat_axis=0, tiled=True)  13.8 us
    all_to_all x2, blocking collectives, sent_to_all(): return lax.all_to_all(copies, axis, split_axis=0, concat_axis=0, tiled=True)  13.4 us
    all_to_all x1, waiting for transfers between devices, per_device(): lax.all_to_all(results, 'ep', split_axis=0, concat_axis=0, tiled=True)  13 us
    mul x2, local copies, waits for them, and re-layouts, per_device(): forget[..., None] * previous  9.72 us
    all_to_all x1, waiting for transfers between devices, per_device(): lax.all_to_all(outgoing, 'ep', split_axis=0, concat_axis=0, tiled=True)  7.58 us
    all_to_all x1, blocking collectives, sent_and_summed(): lax.all_to_all(blocks, axis, split_axis=0, concat_axis=0, tiled=True)  7.25 us
    all_to_all x1, starting transfers between devices, per_device(): lax.all_to_all(results, 'ep', split_axis=0, concat_axis=0, tiled=True)  6.35 us
    add x1, other arithmetic, per_device(): forget[..., None] * previous  6.16 us
  transfers between devices with their start and end apart: 2, of which 2 were waited for; matrix products, arithmetic and copies ran while one was open for 21% of the time, Pallas kernels for 0%

commit v1 on v0

v1 whole, which is shorter than its diff:
```python
import functools

import jax
import jax.numpy as jnp
from jax import lax
from jax.experimental import pallas as pl
from jax.experimental.pallas import tpu as pltpu
from jax.sharding import PartitionSpec as P

MESH = pl.DeviceIdType.MESH
BF = jnp.bfloat16
F32 = jnp.float32


def dot(a, b):
    return jnp.dot(a, b, preferred_element_type=F32)


def silu(v):
    return v / (1.0 + jnp.exp(-v))


def kernel(
    n_ep,
    tokens,
    old,
    w_query,
    w_forget,
    w_value,
    w_gate,
    bound,
    head_gain,
    w_out,
    mix_gain,
    e_gate,
    e_up,
    e_down,
    ids,
    weight,
    moe_gain,
    next_out,
    state_out,
    tok,
    wq,
    wf,
    wv,
    wg,
    st,
    wo,
    eg,
    eu,
    ed,
    f_s,
    q_s,
    v_s,
    r_s,
    mix,
    own_part,
    other_part,
    after,
    send,
    recv_a,
    recv_b,
    down_send,
    down_recv,
    ret_send,
    ret_recv,
    stat_send,
    stat_recv,
    in_sem,
    out_sem,
    tp_send,
    tp_recv,
    ep_send,
    ep_recv,
):
    me = lax.axis_index("ep")
    core = lax.axis_index("tp")
    rows, width = tok.shape
    heads = st.shape[1]
    half = width // 2
    blocks = half // 128
    own_cols = pl.multiple_of(core * half, 128)
    other_cols = pl.multiple_of((1 - core) * half, 128)
    n_slots = 2 * n_ep

    seqs = rows // 3
    loads = [
        pltpu.make_async_copy(src, dst, in_sem.at[i])
        for i, (src, dst) in enumerate(
            (
                (tokens, tok),
                (w_forget, wf),
                (w_value, wv),
                (w_query, wq),
                (old.at[pl.ds(0, seqs)], st.at[pl.ds(0, seqs)]),
                (old.at[pl.ds(seqs, seqs)], st.at[pl.ds(seqs, seqs)]),
                (old.at[pl.ds(2 * seqs, seqs)], st.at[pl.ds(2 * seqs, seqs)]),
                (w_gate, wg),
                (w_out, wo),
                (e_gate.at[0], eg),
                (e_up.at[0], eu),
                (e_down.at[0], ed),
            )
        )
    ]
    for load in loads:
        load.start()

    barrier = pltpu.get_barrier_semaphore()
    pl.semaphore_signal(barrier, inc=1, device_id=(me, 1 - core), device_id_type=MESH)

    def greet(i, carry):
        peer = lax.rem(me + i, n_ep)
        pl.semaphore_signal(barrier, inc=1, device_id=(peer, core), device_id_type=MESH)
        return carry

    lax.fori_loop(1, n_ep, greet, 0)

    slot_iota = lax.broadcasted_iota(jnp.int32, (rows, n_slots), 1)
    expert_iota = lax.shift_right_logical(slot_iota, 1)
    id0 = ids[:, 0:1]
    id1 = ids[:, 1:2]
    names0 = expert_iota == id0
    names1 = expert_iota == id1
    named = jnp.where(names0 | names1, 1.0, 0.0)
    r_iota = lax.broadcasted_iota(jnp.int32, (rows, rows), 0)
    c_iota = lax.broadcasted_iota(jnp.int32, (rows, rows), 1)
    earlier = jnp.where(c_iota < r_iota, 1.0, 0.0)
    rank = dot(earlier.astype(BF), named.astype(BF))
    slot_of = lax.bitwise_and(slot_iota, 1).astype(F32)
    takes = jnp.where(rank == slot_of, named, 0.0)
    route = jnp.where(names0, weight[:, 0:1], 0.0) + jnp.where(names1, weight[:, 1:2], 0.0)
    route = jnp.where(rank == slot_of, route, 0.0)
    route_high = route.astype(BF)
    route_low = (route - route_high.astype(F32)).astype(BF)
    choose = takes.T.astype(BF)

    pairs = heads // 2

    def by_head(ref, values, p):
        ref[pl.ds(2 * p, rows, heads), :] = values
        ref[pl.ds(2 * p + 1, rows, heads), :] = values

    loads[0].wait()
    x = tok[...]
    loads[1].wait()
    f_lin = dot(x, wf[...])
    for p in range(pairs):
        cols = slice(p * 128, (p + 1) * 128)
        low = bound[:, cols]
        by_head(f_s, low + (1.0 - low) / (1.0 + jnp.exp(-f_lin[:, cols])), p)
    loads[2].wait()
    v_lin = dot(x, wv[...])
    for p in range(pairs):
        by_head(v_s, v_lin[:, p * 128 : (p + 1) * 128], p)
    loads[3].wait()
    q_lin = dot(x, wq[...])
    for p in range(pairs):
        by_head(q_s, silu(q_lin[:, p * 128 : (p + 1) * 128]), p)

    lane = lax.broadcasted_iota(jnp.int32, (heads, 128), 1)
    head = lax.broadcasted_iota(jnp.int32, (heads, 128), 0)
    odd = lax.bitwise_and(head, 1) * 64
    key_at = odd + lax.shift_right_logical(lane, 6)
    value_at = odd + lax.bitwise_and(lane, 63)
    n_cols = st.shape[2] // 128

    def one_sequence(s, carry):
        at = pl.ds(pl.multiple_of(s * heads, heads), heads)
        f_row = f_s[at, :]
        q_row = q_s[at, :]
        v_row = jnp.take_along_axis(v_s[at, :], value_at, axis=1)
        sums = [jnp.zeros((heads, 128), F32) for _ in range(4)]
        for c in range(n_cols):
            key = key_at + 2 * c
            f_here = jnp.take_along_axis(f_row, key, axis=1)
            q_here = jnp.take_along_axis(q_row, key, axis=1)
            new = v_row + f_here * (st[s, :, c * 128 : (c + 1) * 128] - v_row)
            st[s, :, c * 128 : (c + 1) * 128] = new
            sums[c % 4] = sums[c % 4] + q_here * new
        total = (sums[0] + sums[1]) + (sums[2] + sums[3])
        r_s[at, :] = total + pltpu.roll(total, 64, 1)
        return carry

    outs = []
    for part in range(3):
        loads[4 + part].wait()
        lax.fori_loop(part * seqs, (part + 1) * seqs, one_sequence, 0)
        out = pltpu.make_async_copy(
            st.at[pl.ds(part * seqs, seqs)],
            state_out.at[pl.ds(part * seqs, seqs)],
            out_sem.at[part],
        )
        out.start()
        outs.append(out)

    loads[7].wait()
    g_lin = dot(x, wg[...])
    first_head = lax.broadcasted_iota(jnp.int32, (rows, 128), 1) < 64
    gain2 = jnp.concatenate([head_gain[...], head_gain[...]], axis=1)
    for p in range(pairs):
        cols = slice(p * 128, (p + 1) * 128)
        even_head = r_s[pl.ds(2 * p, rows, heads), :]
        odd_head = r_s[pl.ds(2 * p + 1, rows, heads), :]
        even_head = even_head * lax.rsqrt(
            jnp.sum(even_head * even_head, -1, keepdims=True) / 128.0 + 1e-6
        )
        odd_head = odd_head * lax.rsqrt(
            jnp.sum(odd_head * odd_head, -1, keepdims=True) / 128.0 + 1e-6
        )
        normed = jnp.where(first_head, even_head, odd_head) * gain2
        mix[:, cols] = (normed * silu(g_lin[:, cols])).astype(BF)
    loads[8].wait()
    own_part[...] = dot(mix[...], wo[...]).astype(BF)

    pl.semaphore_wait(barrier, n_ep)

    def to_partner(src, dst, i):
        return pltpu.make_async_remote_copy(
            src_ref=src,
            dst_ref=dst,
            send_sem=tp_send.at[i],
            recv_sem=tp_recv.at[i],
            device_id=(me, 1 - core),
            device_id_type=MESH,
        )

    swap = to_partner(own_part, other_part, 0)
    swap.start()
    swap.wait()
    mixed = own_part[...].astype(F32) + other_part[...].astype(F32)
    full = x.astype(F32) + mixed
    centered = full - jnp.mean(full, -1, keepdims=True)
    variance = jnp.mean(centered * centered, -1, keepdims=True)
    after[...] = (centered * lax.rsqrt(variance + 1e-5) * mix_gain[...]).astype(BF)

    after_half = after[:, pl.ds(own_cols, half)]
    for j in range(blocks):
        picked = dot(choose, after_half[:, j * 128 : (j + 1) * 128]).astype(BF)
        send[j] = picked.reshape(n_ep, 2, 128)

    def exchange(src, dst, i):
        def one(k, carry):
            peer = lax.rem(me + k, n_ep)
            pltpu.make_async_remote_copy(
                src_ref=src.at[:, peer],
                dst_ref=dst.at[:, me],
                send_sem=ep_send.at[i],
                recv_sem=ep_recv.at[i],
                device_id=(peer, core),
                device_id_type=MESH,
            ).start()
            return carry

        lax.fori_loop(1, n_ep, one, 0)
        dst[:, pl.ds(me, 1)] = src[:, pl.ds(me, 1)]

    def exchanged(src, dst, i):
        whole = pltpu.make_async_remote_copy(
            src_ref=src.at[:, pl.ds(0, n_ep - 1)],
            dst_ref=dst.at[:, pl.ds(0, n_ep - 1)],
            send_sem=ep_send.at[i],
            recv_sem=ep_recv.at[i],
            device_id=(me, 1 - core),
            device_id_type=MESH,
        )
        return whole

    exchange(send, recv_a, 0)
    dispatched = exchanged(send, recv_a, 0)
    dispatched.wait_recv()
    forward = to_partner(recv_a, recv_b, 1)
    forward.start()
    for i in (9, 10, 11):
        loads[i].wait()

    def project(buf, weights, first):
        total = jnp.zeros((n_slots, weights.shape[1]), F32)
        for j in range(blocks):
            total += dot(
                buf[j].reshape(n_slots, 128),
                weights[pl.ds(pl.multiple_of(first + j * 128, 128), 128), :],
            )
        return total

    gate_act = project(recv_a, eg, own_cols)
    up_act = project(recv_a, eu, own_cols)
    forward.wait_recv()
    gate_act += project(recv_b, eg, other_cols)
    up_act += project(recv_b, eu, other_cols)
    hidden = (silu(gate_act) * up_act).astype(BF)

    down_send[...] = dot(hidden, ed[:, pl.ds(other_cols, half)]).astype(BF)
    meet = to_partner(down_send, down_recv, 2)
    meet.start()
    kept = dot(hidden, ed[:, pl.ds(own_cols, half)]).astype(BF).astype(F32)
    meet.wait_recv()
    summed = (kept + down_recv[...].astype(F32)).astype(BF)
    for j in range(blocks):
        ret_send[j] = summed[:, j * 128 : (j + 1) * 128].reshape(n_ep, 2, 128)
    exchange(ret_send, ret_recv, 1)
    returned = exchanged(ret_send, ret_recv, 1)
    returned.wait_recv()

    route_both = jnp.concatenate([route_high.astype(F32), route_low.astype(F32)], axis=0).astype(BF)
    sums = []
    for j in range(blocks):
        both = dot(route_both, ret_recv[j].reshape(n_slots, 128))
        sums.append(both[:rows] + both[rows:])
    moe_sum = jnp.concatenate(sums, axis=1)
    final = after[:, pl.ds(own_cols, half)].astype(F32) + moe_sum
    own_mean = jnp.mean(final, -1, keepdims=True)
    off = final - own_mean
    own_var = jnp.mean(off * off, -1, keepdims=True)
    stat_send[...] = jnp.where(first_head, own_mean, own_var)
    stats = to_partner(stat_send, stat_recv, 3)
    stats.start()
    stats.wait_recv()
    other_mean = stat_recv[:, 0:1]
    other_var = stat_recv[:, 64:65]
    gap = own_mean - other_mean
    mean = 0.5 * (own_mean + other_mean)
    variance = 0.5 * (own_var + other_var) + 0.25 * gap * gap
    gain = moe_gain[:, pl.ds(own_cols, half)]
    next_out[...] = ((final - mean) * lax.rsqrt(variance + 1e-5) * gain).astype(BF)

    for out in outs:
        out.wait()
    dispatched.wait_send()
    returned.wait_send()
    for remote in (forward, meet, stats):
        remote.wait_send()


def per_device(
    tokens,
    old_state,
    w_query,
    w_forget,
    w_value,
    w_gate,
    lower_bound,
    head_gain,
    w_out,
    mix_gain,
    expert_gate,
    expert_up,
    expert_down,
    expert_ids,
    route_weight,
    moe_gain,
):
    n_ep = lax.axis_size("ep")
    rows, width = tokens.shape
    heads = old_state.shape[1]
    cols = w_query.shape[1]
    units = expert_gate.shape[2]
    half = width // 2
    blocks = half // 128
    n_slots = 2 * n_ep
    anywhere = pl.BlockSpec(memory_space=pl.ANY)
    vmem = pl.BlockSpec(memory_space=pltpu.VMEM)
    message = pltpu.VMEM((blocks, n_ep, 2, 128), BF)
    return pl.pallas_call(
        functools.partial(kernel, n_ep),
        out_shape=(
            jax.ShapeDtypeStruct((rows, half), BF),
            jax.ShapeDtypeStruct(old_state.shape, F32),
        ),
        in_specs=[
            anywhere,
            anywhere,
            anywhere,
            anywhere,
            anywhere,
            anywhere,
            vmem,
            vmem,
            anywhere,
            vmem,
            anywhere,
            anywhere,
            anywhere,
            vmem,
            vmem,
            vmem,
        ],
        out_specs=(vmem, anywhere),
        scratch_shapes=[
            pltpu.VMEM((rows, width), BF),
            pltpu.VMEM((width, cols), BF),
            pltpu.VMEM((width, cols), BF),
            pltpu.VMEM((width, cols), BF),
            pltpu.VMEM((width, cols), BF),
            pltpu.VMEM(old_state.shape, F32),
            pltpu.VMEM((cols, width), BF),
            pltpu.VMEM((width, units), BF),
            pltpu.VMEM((width, units), BF),
            pltpu.VMEM((units, width), BF),
            pltpu.VMEM((rows * heads, 128), F32),
            pltpu.VMEM((rows * heads, 128), F32),
            pltpu.VMEM((rows * heads, 128), F32),
            pltpu.VMEM((rows * heads, 128), F32),
            pltpu.VMEM((rows, cols), BF),
            pltpu.VMEM((rows, width), BF),
            pltpu.VMEM((rows, width), BF),
            pltpu.VMEM((rows, width), BF),
            message,
            message,
            message,
            pltpu.VMEM((n_slots, half), BF),
            pltpu.VMEM((n_slots, half), BF),
            message,
            message,
            pltpu.VMEM((rows, 128), F32),
            pltpu.VMEM((rows, 128), F32),
            pltpu.SemaphoreType.DMA((12,)),
            pltpu.SemaphoreType.DMA((3,)),
            pltpu.SemaphoreType.DMA((4,)),
            pltpu.SemaphoreType.DMA((4,)),
            pltpu.SemaphoreType.DMA((2,)),
            pltpu.SemaphoreType.DMA((2,)),
        ],
        compiler_params=pltpu.CompilerParams(
            collective_id=0, has_side_effects=True, vmem_limit_bytes=56 * 1024 * 1024
        ),
    )(
        tokens,
        old_state,
        w_query,
        w_forget,
        w_value,
        w_gate,
        lower_bound.reshape(1, cols),
        head_gain.reshape(1, -1),
        w_out,
        mix_gain.reshape(1, width),
        expert_gate,
        expert_up,
        expert_down,
        expert_ids,
        route_weight,
        moe_gain.reshape(1, width),
    )


def solution(mesh):
    in_specs = (
        P("ep", None),
        P("ep", "tp", None),
        P(None, "tp"),
        P(None, "tp"),
        P(None, "tp"),
        P(None, "tp"),
        P("tp"),
        P(),
        P("tp", None),
        P(),
        P("ep", None, "tp"),
        P("ep", None, "tp"),
        P("ep", "tp", None),
        P("ep", None),
        P("ep", None),
        P(),
    )
    out_specs = (P("ep", "tp"), P("ep", "tp", None))
    return jax.shard_map(
        per_device, mesh=mesh, in_specs=in_specs, out_specs=out_specs, check_vma=False
    )
```

time: 131 us -> 67.2 us (0.51)
  Pallas kernels: 0 us -> 58.3 us
  local copies, waits for them, and re-layouts: 33.7 us -> 7.99 us
  blocking collectives: 20.7 us -> 0 us
  waiting for transfers between devices: 20.6 us -> 0 us
  starting transfers between devices: 20.2 us -> 0 us
  matrix products: 18.5 us -> 0 us
  other arithmetic: 15.2 us -> 0 us
    pallas_call x0 -> x1, Pallas kernels: none -> 58.3 us  [per_device(): pl.pallas_call(functools.partial(kernel, n_ep), out_shape=(jax.ShapeDtype...]
    all_to_all x3 -> x0, blocking collectives: 20.7 us -> none  [the longest x2 13.4 us: sent_to_all(): return lax.all_to_all(copies, axis, split_axis=0, concat_axis=0, tiled=True)]
    all_to_all x2 -> x0, waiting for transfers between devices: 20.6 us -> none  [the longest x1 13 us: per_device(): lax.all_to_all(results, 'ep', split_axis=0, concat_axis=0, tiled=True)]
    all_to_all x2 -> x0, starting transfers between devices: 20.2 us -> none  [the longest x1 13.8 us: per_device(): lax.all_to_all(outgoing, 'ep', split_axis=0, concat_axis=0, tiled=True)]
    dot_general x9 -> x0, matrix products: 18.5 us -> none  [the longest x1 6.04 us: per_device(): readout = jnp.einsum('shi,shij->shj', act_query, new_state)]
    mul x6 -> x0, local copies, waits for them, and re-layouts: 16.3 us -> none  [the longest x2 9.72 us: per_device(): forget[..., None] * previous]
    reshape x8 -> x0, local copies, waits for them, and re-layouts: 11.2 us -> none  [the longest x1 6.14 us: per_device(): previous = old_state.reshape(row_count, heads_here, head_dim, head_dim)]
    unnamed x21 -> x4, local copies, waits for them, and re-layouts: 1.16 us -> 7.99 us
  transfers between devices with their start and end apart: 2 -> 0, of which waited for: 2 -> 0; matrix products, arithmetic and copies ran while one was open for 21% -> 0% of each run, Pallas kernels for 0% -> 0%
where the time goes in v1:
time: 67.2 us; the launch traced here: 66.9 us
  Pallas kernels  58.3 us (87%)
  local copies, waits for them, and re-layouts  7.99 us (12%)
    pallas_call x1, Pallas kernels, per_device(): pl.pallas_call(functools.partial(kernel, n_ep), out_shape=(jax.ShapeDtype...  58.3 us
    unnamed x4, local copies, waits for them, and re-layouts  7.99 us

profile of v1, /device:TPU:1, one launch (start us, length us, event | category | flops | bytes accessed | tf_op | source)
XLA Modules:
  0.0 66.9 jit_solution(15833222887825701952)
XLA Ops:
  0.6 1.4 %copy.18.ids = s32[24,2]{1,0:T(8,128)} copy(s32[24,2]{0,1:T(2,128)} %param.29) | data formatting | bytes 384 | tf_op args[13]
  2.0 1.4 %copy.19.weight = f32[24,2]{1,0:T(8,128)} copy(f32[24,2]{0,1:T(2,128)} %param.30) | data formatting | bytes 384 | tf_op args[14]
  3.3 58.3 %shard_map.167 = (bf16[24,1024]{1,0:T(8,128)(2,1)}, f32[24,8,4096]{2,1,0:T(8,128)}) custom-call(bf16[24,2048]{1,0:T(8,128)(2,1)} %tokens.1, f32[24,8,4096]{2,1,0:T(8,128)} %old.1, bf16[2048,512]{1,0:T(8,128)(2,1)} %w_query.1, bf16[2048,512]{1,0:T(8,128)(2,1)} %w_forget.1, bf16[2048,512]{1,0:T(8,128)(2,1)} %w_value.1, bf16[2048,512]{1,0:T(8,128)(2,1)} %w_gate.1, ...), custom_call_target="tpu_custom_call" | custom-call | tf_op jit(solution)/shard_map/pallas_call | solution.py:365
  61.7 1.4 %copy.22 = bf16[24,1024]{1,0:T(8,128)(2,1)} copy(bf16[24,1024]{1,0:T(8,128)(2,1)} %get-tuple-element.4) | data formatting | bytes 98304
  63.1 3.9 %copy.23 = f32[24,8,4096]{2,1,0:T(8,128)} copy(f32[24,8,4096]{2,1,0:T(8,128)} %get-tuple-element.5) | data formatting | bytes 6291456

commit v2 on v1

v2 whole, which is shorter than its diff:
```python
import jax
import jax.numpy as jnp
from jax import lax
from jax.experimental import pallas as pl
from jax.experimental.pallas import tpu as pltpu
from jax.sharding import PartitionSpec as P

MESH = pl.DeviceIdType.MESH
BF = jnp.bfloat16
F32 = jnp.float32


def dot(a, b):
    return jnp.dot(a, b, preferred_element_type=F32)


def silu(v):
    return v / (1.0 + jnp.exp(-v))


AXES = (8, 4, 4)
PLANE = AXES[1] * AXES[2]
Z_ORDER = (4, 3, 5, 2, 6, 1, 7, 0)
GROUPS = ((0, 1), (1, 3), (3, 5), (5, 8))
SELF = 7 * PLANE


def kernel(
    tokens,
    old,
    w_query,
    w_forget,
    w_value,
    w_gate,
    bound_in,
    head_gain_in,
    w_out,
    mix_gain_in,
    e_gate,
    e_up,
    e_down,
    ids_in,
    weight_in,
    moe_gain_in,
    next_out,
    st,
    tok,
    wq,
    wf,
    wv,
    wg,
    wo,
    eg,
    eu,
    ed,
    bound,
    head_gain,
    mix_gain,
    ids,
    weight,
    moe_gain,
    f_s,
    q_s,
    v_s,
    r_s,
    gates,
    mix,
    own_part,
    other_part,
    after,
    send,
    recv_a,
    recv_b,
    down_keep,
    down_send,
    down_recv,
    ret_send,
    ret_recv,
    stat_send,
    stat_recv,
    small,
    in_sem,
    tp_send,
    tp_recv,
    ep_send,
    ep_recv,
):
    me = lax.axis_index("ep")
    core = lax.axis_index("tp")
    n_ep = AXES[0] * PLANE
    rows, width = tok.shape
    heads = st.shape[1]
    half = width // 2
    blocks = half // 128
    own_cols = pl.multiple_of(core * half, 128)
    other_cols = pl.multiple_of((1 - core) * half, 128)
    n_slots = 2 * n_ep
    n_keys = st.shape[2]
    my_z = lax.div(me, PLANE)
    my_y = lax.rem(lax.div(me, AXES[2]), AXES[1])
    my_x = lax.rem(me, AXES[2])

    def at_offset(dz, r, sign):
        dy = lax.div(r, AXES[2])
        dx = lax.rem(r, AXES[2])
        if sign < 0:
            dz, dy, dx = AXES[0] - dz, AXES[1] - dy, AXES[2] - dx
        return (
            lax.rem(my_z + dz, AXES[0]) * PLANE
            + lax.rem(my_y + dy, AXES[1]) * AXES[2]
            + lax.rem(my_x + dx, AXES[2])
        )

    part = n_keys // 4
    pieces = [
        (tokens, tok),
        (bound_in, bound),
        (w_forget, wf),
        (w_query, wq),
        (w_value, wv),
        *((old.at[:, :, pl.ds(i * part, part)], st.at[:, :, pl.ds(i * part, part)]) for i in range(4)),
        (w_gate, wg),
        (head_gain_in, head_gain),
        (w_out, wo),
        (mix_gain_in, mix_gain),
        (ids_in, ids),
        (weight_in, weight),
        (e_gate.at[0], eg),
        (e_up.at[0], eu),
        (e_down.at[0], ed),
        (moe_gain_in, moe_gain),
    ]
    loads = [pltpu.make_async_copy(src, dst, in_sem.at[i]) for i, (src, dst) in enumerate(pieces)]
    for load in loads:
        load.start()
    l_tok, l_bound, l_wf, l_wq, l_wv = loads[:5]
    l_state = loads[5:9]
    l_wg, l_hg, l_wo, l_mg, l_ids, l_weight, l_eg, l_eu, l_ed, l_og = loads[9:]

    barrier = pltpu.get_barrier_semaphore()
    pl.semaphore_signal(barrier, inc=1, device_id=(me, 1 - core), device_id_type=MESH)
    for pos, dz in enumerate(Z_ORDER):

        def greet(r, carry, dz=dz):
            peer = at_offset(dz, r, 1)
            pl.semaphore_signal(barrier, inc=1, device_id=(peer, core), device_id_type=MESH)
            return carry

        lax.fori_loop(1 if dz == 0 else 0, PLANE, greet, 0)

    pairs = heads // 2
    tall = rows * heads

    def by_head(ref, values, p):
        ref[pl.ds(2 * p, rows, heads), :] = values
        ref[pl.ds(2 * p + 1, rows, heads), :] = values

    lane = lax.broadcasted_iota(jnp.int32, (tall, 128), 1)
    head = lax.broadcasted_iota(jnp.int32, (tall, 128), 0)
    mine = lax.shift_right_logical(lane, 6) == lax.bitwise_and(head, 1)

    def split(ref, first):
        values = jnp.where(mine, ref[...], 0.0)
        high = values.astype(BF)
        gates[first : first + tall, 0:128] = high
        gates[first : first + tall, 128:256] = (values - high.astype(F32)).astype(BF)

    l_tok.wait()
    x = tok[...]
    l_bound.wait()
    l_wf.wait()
    f_lin = dot(x, wf[...])
    for p in range(pairs):
        cols = slice(p * 128, (p + 1) * 128)
        low = bound[:, cols]
        by_head(f_s, low + (1.0 - low) / (1.0 + jnp.exp(-f_lin[:, cols])), p)
    split(f_s, 0)
    l_wq.wait()
    q_lin = dot(x, wq[...])
    for p in range(pairs):
        by_head(q_s, silu(q_lin[:, p * 128 : (p + 1) * 128]), p)
    split(q_s, tall)
    l_wv.wait()
    v_lin = dot(x, wv[...])
    for p in range(pairs):
        by_head(v_s, v_lin[:, p * 128 : (p + 1) * 128], p)
    v_pair = v_s[...]
    v_s[...] = jnp.where(mine, v_pair, pltpu.roll(v_pair, 64, 1))
    r_s[...] = jnp.zeros_like(r_s)

    tile = 256
    key_gap = (
        lax.bitwise_and(lax.broadcasted_iota(jnp.int32, (tile, tile), 0), 63)
        - lax.shift_right_logical(lax.broadcasted_iota(jnp.int32, (tile, tile), 1), 6)
    ).astype(F32)

    def one_tile(n, carry):
        spread = jnp.where(key_gap == (4 * n).astype(F32), 1.0, 0.0).astype(BF)
        both = dot(gates[...], spread)
        cols = pl.ds(pl.multiple_of(n * tile, tile), tile)
        previous = st[:, :, cols].reshape(tall, tile)
        value = jnp.concatenate([v_s[...], v_s[...]], axis=1)
        new = value + both[:tall] * (previous - value)
        st[:, :, cols] = new.reshape(rows, heads, tile)
        read = both[tall:] * new
        r_s[...] += read[:, :128] + read[:, 128:]
        return carry

    per_part = part // tile
    for i in range(4):
        l_state[i].wait()
        lax.fori_loop(i * per_part, (i + 1) * per_part, one_tile, 0)
    r_s[...] += pltpu.roll(r_s[...], 64, 1)

    l_wg.wait()
    l_hg.wait()
    g_lin = dot(x, wg[...])
    first_head = lax.broadcasted_iota(jnp.int32, (rows, 128), 1) < 64
    gain2 = jnp.concatenate([head_gain[...], head_gain[...]], axis=1)
    for p in range(pairs):
        cols = slice(p * 128, (p + 1) * 128)
        even_head = r_s[pl.ds(2 * p, rows, heads), :]
        odd_head = r_s[pl.ds(2 * p + 1, rows, heads), :]
        even_head = even_head * lax.rsqrt(
            jnp.sum(even_head * even_head, -1, keepdims=True) / 128.0 + 1e-6
        )
        odd_head = odd_head * lax.rsqrt(
            jnp.sum(odd_head * odd_head, -1, keepdims=True) / 128.0 + 1e-6
        )
        normed = jnp.where(first_head, even_head, odd_head) * gain2
        mix[:, cols] = (normed * silu(g_lin[:, cols])).astype(BF)
    l_wo.wait()
    own_part[...] = dot(mix[...], wo[...]).astype(BF)

    pl.semaphore_wait(barrier, n_ep)

    def to_partner(src, dst, i):
        return pltpu.make_async_remote_copy(
            src_ref=src,
            dst_ref=dst,
            send_sem=tp_send.at[i],
            recv_sem=tp_recv.at[i],
            device_id=(me, 1 - core),
            device_id_type=MESH,
        )

    swap = to_partner(own_part, other_part, 0)
    swap.start()

    for load in (l_ids, l_weight, l_mg):
        load.wait()
    small[...] = jnp.zeros_like(small)
    small[0:2, 0:rows] = ids[...].astype(F32)
    small[2:4, 0:rows] = weight[...]
    turned = small[...].T[0:rows]
    id0 = turned[:, 0:1].astype(jnp.int32)
    id1 = turned[:, 1:2].astype(jnp.int32)
    slot_iota = lax.broadcasted_iota(jnp.int32, (rows, n_slots), 1)
    slot_pos = lax.shift_right_logical(slot_iota, 5)
    dz = jnp.zeros_like(slot_pos)
    for pos, offset in enumerate(Z_ORDER):
        dz = jnp.where(slot_pos == pos, offset, dz)
    dy = lax.bitwise_and(lax.shift_right_logical(slot_iota, 3), 3)
    dx = lax.bitwise_and(lax.shift_right_logical(slot_iota, 1), 3)
    expert = (
        lax.bitwise_and(my_z + dz, 7) * PLANE
        + lax.bitwise_and(my_y + dy, 3) * AXES[2]
        + lax.bitwise_and(my_x + dx, 3)
    )
    names0 = expert == id0
    names1 = expert == id1
    named = jnp.where(names0 | names1, 1.0, 0.0)
    r_iota = lax.broadcasted_iota(jnp.int32, (rows, rows), 0)
    c_iota = lax.broadcasted_iota(jnp.int32, (rows, rows), 1)
    earlier = jnp.where(c_iota < r_iota, 1.0, 0.0)
    rank = dot(earlier.astype(BF), named.astype(BF))
    slot_of = lax.bitwise_and(slot_iota, 1).astype(F32)
    takes = jnp.where(rank == slot_of, named, 0.0)
    route = jnp.where(names0, turned[:, 2:3], 0.0) + jnp.where(names1, turned[:, 3:4], 0.0)
    route = jnp.where(rank == slot_of, route, 0.0)
    route_high = route.astype(BF)
    route_low = (route - route_high.astype(F32)).astype(BF)
    route_both = jnp.concatenate([route_high.astype(F32), route_low.astype(F32)], axis=0).astype(BF)
    choose = takes.T.astype(BF)
    swap.wait()
    mixed = own_part[...].astype(F32) + other_part[...].astype(F32)
    full = x.astype(F32) + mixed
    centered = full - jnp.mean(full, -1, keepdims=True)
    variance = jnp.mean(centered * centered, -1, keepdims=True)
    after[...] = (centered * lax.rsqrt(variance + 1e-5) * mix_gain[...]).astype(BF)

    def exchange(src, dst, send_sem, recv_sem, group, sign):
        for pos in range(*group):

            def one(r, carry, pos=pos):
                k = pos * PLANE + r
                pltpu.make_async_remote_copy(
                    src_ref=src.at[:, k],
                    dst_ref=dst.at[:, k],
                    send_sem=send_sem,
                    recv_sem=recv_sem,
                    device_id=(at_offset(Z_ORDER[pos], r, sign), core),
                    device_id_type=MESH,
                ).start()
                return carry

            lax.fori_loop(1 if pos == 7 else 0, PLANE, one, 0)
        if group[1] == 8:
            dst[:, SELF : SELF + 1] = src[:, SELF : SELF + 1]

    def bytes_of(src, dst, send_sem, recv_sem, first, count):
        return pltpu.make_async_remote_copy(
            src_ref=src.at[:, pl.ds(first, count)],
            dst_ref=dst.at[:, pl.ds(first, count)],
            send_sem=send_sem,
            recv_sem=recv_sem,
            device_id=(me, 1 - core),
            device_id_type=MESH,
        )

    def arrived(src, dst, send_sem, recv_sem, group):
        first, last = group[0] * PLANE, group[1] * PLANE
        count = last - first - (1 if group[1] == 8 else 0)
        bytes_of(src, dst, send_sem, recv_sem, first, count).wait_recv()

    after_half = after[:, pl.ds(own_cols, half)]
    for g, group in enumerate(GROUPS):
        first, last = group[0] * PLANE, group[1] * PLANE
        picked = dot(choose[2 * first : 2 * last], after_half).astype(BF)
        for j in range(blocks):
            send[j, first:last] = picked[:, j * 128 : (j + 1) * 128].reshape(last - first, 2, 128)
        exchange(send, recv_a, ep_send.at[0], ep_recv.at[g], group, 1)

    for load in (l_eg, l_eu, l_ed, l_og):
        load.wait()

    def project(buf, weights, first_row, first, last):
        total = None
        for j in range(blocks):
            term = dot(
                buf[j, first:last].reshape(2 * (last - first), 128),
                weights[pl.ds(pl.multiple_of(first_row + j * 128, 128), 128), :],
            )
            total = term if total is None else total + term
        return total

    forwards = []
    meets = []

    def arrive(g):
        group = GROUPS[g]
        first, last = group[0] * PLANE, group[1] * PLANE
        arrived(send, recv_a, ep_send.at[0], ep_recv.at[g], group)
        forward = to_partner(recv_a.at[:, pl.ds(first, last - first)], recv_b.at[:, pl.ds(first, last - first)], 2 + g)
        forward.start()
        forwards.append(forward)

    def compute(g):
        group = GROUPS[g]
        first, last = group[0] * PLANE, group[1] * PLANE
        at = slice(2 * first, 2 * last)
        gate_act = project(recv_a, eg, own_cols, first, last)
        up_act = project(recv_a, eu, own_cols, first, last)
        forwards[g].wait_recv()
        gate_act += project(recv_b, eg, other_cols, first, last)
        up_act += project(recv_b, eu, other_cols, first, last)
        hidden = (silu(gate_act) * up_act).astype(BF)
        down_send[at] = dot(hidden, ed[:, pl.ds(other_cols, half)]).astype(BF)
        meet = to_partner(
            down_send.at[pl.ds(2 * first, 2 * (last - first))],
            down_recv.at[pl.ds(2 * first, 2 * (last - first))],
            6 + g,
        )
        meet.start()
        meets.append(meet)
        down_keep[at] = dot(hidden, ed[:, pl.ds(own_cols, half)]).astype(BF)

    def give_back(g):
        group = GROUPS[g]
        first, last = group[0] * PLANE, group[1] * PLANE
        at = slice(2 * first, 2 * last)
        meets[g].wait_recv()
        summed = (down_keep[at].astype(F32) + down_recv[at].astype(F32)).astype(BF)
        for j in range(blocks):
            ret_send[j, first:last] = summed[:, j * 128 : (j + 1) * 128].reshape(last - first, 2, 128)
        exchange(ret_send, ret_recv, ep_send.at[1], ep_recv.at[4 + g], group, -1)

    for g in range(len(GROUPS)):
        arrive(g)
        if g > 0:
            give_back(g - 1)
        compute(g)
    give_back(len(GROUPS) - 1)

    moe_sum = None
    for g, group in enumerate(GROUPS):
        first, last = group[0] * PLANE, group[1] * PLANE
        arrived(ret_send, ret_recv, ep_send.at[1], ep_recv.at[4 + g], group)
        sums = []
        for j in range(blocks):
            sums.append(
                dot(
                    route_both[:, 2 * first : 2 * last],
                    ret_recv[j, first:last].reshape(2 * (last - first), 128),
                )
            )
        both = jnp.concatenate(sums, axis=1)
        both = both[:rows] + both[rows:]
        moe_sum = both if moe_sum is None else moe_sum + both
    final = after[:, pl.ds(own_cols, half)].astype(F32) + moe_sum
    own_mean = jnp.mean(final, -1, keepdims=True)
    off = final - own_mean
    own_var = jnp.mean(off * off, -1, keepdims=True)
    stat_send[...] = jnp.where(first_head, own_mean, own_var)
    stats = to_partner(stat_send, stat_recv, 1)
    stats.start()
    stats.wait_recv()
    other_mean = stat_recv[:, 0:1]
    other_var = stat_recv[:, 64:65]
    gap = own_mean - other_mean
    mean = 0.5 * (own_mean + other_mean)
    variance = 0.5 * (own_var + other_var) + 0.25 * gap * gap
    gain = moe_gain[:, pl.ds(own_cols, half)]
    next_out[...] = ((final - mean) * lax.rsqrt(variance + 1e-5) * gain).astype(BF)

    bytes_of(send, recv_a, ep_send.at[0], ep_recv.at[0], 0, n_ep - 1).wait_send()
    bytes_of(ret_send, ret_recv, ep_send.at[1], ep_recv.at[4], 0, n_ep - 1).wait_send()
    for remote in (*forwards, *meets, stats):
        remote.wait_send()


def per_device(
    tokens,
    old_state,
    w_query,
    w_forget,
    w_value,
    w_gate,
    lower_bound,
    head_gain,
    w_out,
    mix_gain,
    expert_gate,
    expert_up,
    expert_down,
    expert_ids,
    route_weight,
    moe_gain,
):
    n_ep = lax.axis_size("ep")
    rows, width = tokens.shape
    heads = old_state.shape[1]
    cols = w_query.shape[1]
    units = expert_gate.shape[2]
    half = width // 2
    blocks = half // 128
    n_slots = 2 * n_ep
    tall = rows * heads
    anywhere = pl.BlockSpec(memory_space=pl.ANY)
    vmem = pl.BlockSpec(memory_space=pltpu.VMEM)
    message = pltpu.VMEM((blocks, n_ep, 2, 128), BF)
    down = pltpu.VMEM((n_slots, half), BF)
    by_head = pltpu.VMEM((tall, 128), F32)
    row = pltpu.VMEM((rows, width), BF)
    return pl.pallas_call(
        kernel,
        out_shape=(
            pltpu.VMEM((rows, half), BF),
            pltpu.VMEM(old_state.shape, F32),
        ),
        in_specs=[anywhere] * 16,
        out_specs=(vmem, vmem),
        scratch_shapes=[
            row,
            *[pltpu.VMEM((width, cols), BF)] * 4,
            pltpu.VMEM((cols, width), BF),
            pltpu.VMEM((width, units), BF),
            pltpu.VMEM((width, units), BF),
            pltpu.VMEM((units, width), BF),
            pltpu.VMEM((1, cols), F32),
            pltpu.VMEM((1, head_gain.shape[0]), F32),
            pltpu.VMEM((1, width), F32),
            pltpu.VMEM((2, rows), jnp.int32),
            pltpu.VMEM((2, rows), F32),
            pltpu.VMEM((1, width), F32),
            by_head,
            by_head,
            by_head,
            by_head,
            pltpu.VMEM((2 * tall, 256), BF),
            pltpu.VMEM((rows, cols), BF),
            row,
            row,
            row,
            message,
            message,
            message,
            down,
            down,
            down,
            message,
            message,
            pltpu.VMEM((rows, 128), F32),
            pltpu.VMEM((rows, 128), F32),
            pltpu.VMEM((8, 128), F32),
            pltpu.SemaphoreType.DMA((19,)),
            pltpu.SemaphoreType.DMA((10,)),
            pltpu.SemaphoreType.DMA((10,)),
            pltpu.SemaphoreType.DMA((2,)),
            pltpu.SemaphoreType.DMA((8,)),
        ],
        compiler_params=pltpu.CompilerParams(
            collective_id=0, has_side_effects=True, vmem_limit_bytes=56 * 1024 * 1024
        ),
    )(
        tokens,
        old_state,
        w_query,
        w_forget,
        w_value,
        w_gate,
        lower_bound.reshape(1, cols),
        head_gain.reshape(1, -1),
        w_out,
        mix_gain.reshape(1, width),
        expert_gate,
        expert_up,
        expert_down,
        expert_ids.T,
        route_weight.T,
        moe_gain.reshape(1, width),
    )


def solution(mesh):
    in_specs = (
        P("ep", None),
        P("ep", "tp", None),
        P(None, "tp"),
        P(None, "tp"),
        P(None, "tp"),
        P(None, "tp"),
        P("tp"),
        P(),
        P("tp", None),
        P(),
        P("ep", None, "tp"),
        P("ep", None, "tp"),
        P("ep", "tp", None),
        P("ep", None),
        P("ep", None),
        P(),
    )
    out_specs = (P("ep", "tp"), P("ep", "tp", None))
    return jax.shard_map(
        per_device, mesh=mesh, in_specs=in_specs, out_specs=out_specs, check_vma=False
    )
```

time: 67.2 us -> 52 us (0.77)
  Pallas kernels: 58.3 us -> 49 us
  local copies, waits for them, and re-layouts: 7.99 us -> 2.29 us
    pallas_call x1, Pallas kernels: 58.3 us -> 49 us  [per_device(): pl.pallas_call(kernel, out_shape=(pltpu.VMEM((rows, half), BF), pltpu.VME...]
    unnamed x4 -> x2, local copies, waits for them, and re-layouts: 7.99 us -> 2.29 us
where the time goes in v2:
time: 52 us; the launch traced here: 51.9 us
  Pallas kernels  49 us (94%)
  local copies, waits for them, and re-layouts  2.29 us (4%)
  between operations  0.65 us (1%)
    pallas_call x1, Pallas kernels, per_device(): pl.pallas_call(kernel, out_shape=(pltpu.VMEM((rows, half), BF), pltpu.VME...  49 us
    unnamed x2, local copies, waits for them, and re-layouts  2.29 us

profile of v2, /device:TPU:1, one launch (start us, length us, event | category | flops | bytes accessed | tf_op | source)
XLA Modules:
  0.0 51.9 jit_solution(12865616841189533218)
XLA Ops:
  0.6 49.0 %shard_map.167 = (bf16[24,1024]{1,0:T(8,128)(2,1)S(1)}, f32[24,8,4096]{2,1,0:T(8,128)S(1)}) custom-call(bf16[24,2048]{1,0:T(8,128)(2,1)} %tokens.1, f32[24,8,4096]{2,1,0:T(8,128)} %old.1, bf16[2048,512]{1,0:T(8,128)(2,1)} %w_query.1, bf16[2048,512]{1,0:T(8,128)(2,1)} %w_forget.1, bf16[2048,512]{1,0:T(8,128)(2,1)} %w_value.1, bf16[2048,512]{1,0:T(8,128)(2,1)} %w_gate.1, ...), custom_call_target="tpu_custom_call" | custom-call | tf_op jit(solution)/shard_map/pallas_call | solution.py:465
  49.6 0.6 %copy.20 = bf16[24,1024]{1,0:T(8,128)(2,1)} copy(bf16[24,1024]{1,0:T(8,128)(2,1)S(1)} %get-tuple-element.2) | data formatting | bytes 98304
  50.2 1.7 %copy.21 = f32[24,8,4096]{2,1,0:T(8,128)} copy(f32[24,8,4096]{2,1,0:T(8,128)S(1)} %get-tuple-element.3) | data formatting | bytes 6291456

commit v3 on v2

v3 whole, which is shorter than its diff:
```python
import jax
import jax.numpy as jnp
from jax import lax
from jax.experimental import pallas as pl
from jax.experimental.pallas import tpu as pltpu
from jax.sharding import PartitionSpec as P

MESH = pl.DeviceIdType.MESH
BF = jnp.bfloat16
F32 = jnp.float32


def dot(a, b):
    return jnp.dot(a, b, preferred_element_type=F32)


def silu(v):
    return v / (1.0 + jnp.exp(-v))


AXES = (8, 4, 4)
CHIPS = AXES[1] * AXES[2]
PLANE = CHIPS // 2
Z_ORDER = (3, 5, 2, 6, 4, 1, 7, 0)
GROUPS = ((0, 2), (2, 4), (4, 5), (5, 8))
HOME = Z_ORDER.index(0)
SELF = HOME * PLANE


def kernel(
    tokens,
    old,
    w_query,
    w_forget,
    w_value,
    w_gate,
    bound_in,
    head_gain_in,
    w_out,
    mix_gain_in,
    e_gate,
    e_up,
    e_down,
    ids_in,
    weight_in,
    moe_gain_in,
    next_out,
    st,
    tok,
    wq,
    wf,
    wv,
    wg,
    wo,
    eg,
    eu,
    ed,
    eg_far,
    eu_far,
    ed_far,
    bound,
    head_gain,
    mix_gain,
    ids,
    weight,
    moe_gain,
    f_s,
    q_s,
    v_s,
    r_s,
    gates,
    mix,
    own_part,
    other_part,
    after,
    send,
    recv,
    ret_send,
    ret_recv,
    own_moe,
    other_moe,
    small,
    in_sem,
    tp_send,
    tp_recv,
    ep_send,
    ep_recv,
):
    me = lax.axis_index("ep")
    core = lax.axis_index("tp")
    rows, width = tok.shape
    heads = st.shape[1]
    half = width // 2
    blocks = width // 128
    own_cols = pl.multiple_of(core * half, 128)
    slots = AXES[0] * PLANE
    n_keys = st.shape[2]
    my_z = lax.div(me, CHIPS)
    my_y = lax.rem(lax.div(me, AXES[2]), AXES[1])
    my_x = lax.rem(me, AXES[2])
    z_at = [lax.rem(my_z + dz, AXES[0]) * CHIPS for dz in range(AXES[0])]
    x_at = {
        (sign, q): lax.rem(my_x + AXES[2] + sign * (2 * q + core), AXES[2])
        for sign in (1, -1)
        for q in (0, 1)
    }

    def each_of_plane(pos, sign, visit):
        dz = Z_ORDER[pos]
        base = z_at[(sign * dz) % AXES[0]]

        def one(dy, q):
            y = my_y + dy if sign > 0 else my_y + AXES[1] - dy
            y = jnp.where(y >= AXES[1], y - AXES[1], y) * AXES[2]
            visit(pos * PLANE + dy * 2 + q, base + y + x_at[sign, q])

        def body(dy, carry):
            one(dy, 0)
            one(dy, 1)
            return carry

        if dz == 0:

            @pl.when(core == 1)
            def _():
                one(0, 0)

            one(0, 1)
        lax.fori_loop(1 if dz == 0 else 0, AXES[1], body, 0)

    part = n_keys // 4
    pieces = [
        (tokens, tok),
        (bound_in, bound),
        (w_forget, wf),
        (w_query, wq),
        (w_value, wv),
        *((old.at[:, :, pl.ds(i * part, part)], st.at[:, :, pl.ds(i * part, part)]) for i in range(4)),
        (w_gate, wg),
        (head_gain_in, head_gain),
        (w_out, wo),
        (mix_gain_in, mix_gain),
        (ids_in, ids),
        (weight_in, weight),
        (e_gate.at[0], eg),
        (e_up.at[0], eu),
        (e_down.at[0], ed),
        (moe_gain_in, moe_gain),
    ]
    loads = [pltpu.make_async_copy(src, dst, in_sem.at[i]) for i, (src, dst) in enumerate(pieces)]
    for load in loads:
        load.start()
    l_tok, l_bound, l_wf, l_wq, l_wv = loads[:5]
    l_state = loads[5:9]
    l_wg, l_hg, l_wo, l_mg, l_ids, l_weight, l_eg, l_eu, l_ed, l_og = loads[9:]

    barrier = pltpu.get_barrier_semaphore()
    pl.semaphore_signal(barrier, inc=1, device_id=(me, 1 - core), device_id_type=MESH)

    def greet(slot, peer):
        pl.semaphore_signal(barrier, inc=1, device_id=(peer, core), device_id_type=MESH)

    for dz in (4, 3, 5, 2, 6, 1, 7, 0):
        each_of_plane(Z_ORDER.index(dz), 1, greet)

    pairs = heads // 2
    tall = rows * heads

    def by_head(ref, values, p):
        ref[pl.ds(2 * p, rows, heads), :] = values
        ref[pl.ds(2 * p + 1, rows, heads), :] = values

    lane = lax.broadcasted_iota(jnp.int32, (tall, 128), 1)
    head = lax.broadcasted_iota(jnp.int32, (tall, 128), 0)
    mine = lax.shift_right_logical(lane, 6) == lax.bitwise_and(head, 1)

    def split(ref, first):
        values = jnp.where(mine, ref[...], 0.0)
        high = values.astype(BF)
        gates[first : first + tall, 0:128] = high
        gates[first : first + tall, 128:256] = (values - high.astype(F32)).astype(BF)

    l_tok.wait()
    x = tok[...]
    l_bound.wait()
    l_wf.wait()
    f_lin = dot(x, wf[...])
    for p in range(pairs):
        cols = slice(p * 128, (p + 1) * 128)
        low = bound[:, cols]
        by_head(f_s, low + (1.0 - low) / (1.0 + jnp.exp(-f_lin[:, cols])), p)
    split(f_s, 0)
    l_wq.wait()
    q_lin = dot(x, wq[...])
    for p in range(pairs):
        by_head(q_s, silu(q_lin[:, p * 128 : (p + 1) * 128]), p)
    split(q_s, tall)
    l_wv.wait()
    v_lin = dot(x, wv[...])
    for p in range(pairs):
        by_head(v_s, v_lin[:, p * 128 : (p + 1) * 128], p)
    v_pair = v_s[...]
    v_s[...] = jnp.where(mine, v_pair, pltpu.roll(v_pair, 64, 1))
    r_s[...] = jnp.zeros_like(r_s)

    tile = 256
    key_gap = (
        lax.bitwise_and(lax.broadcasted_iota(jnp.int32, (tile, tile), 0), 63)
        - lax.shift_right_logical(lax.broadcasted_iota(jnp.int32, (tile, tile), 1), 6)
    ).astype(F32)

    def one_tile(n):
        spread = jnp.where(key_gap == 4.0 * n, 1.0, 0.0).astype(BF)
        both = dot(gates[...], spread)
        cols = slice(n * tile, (n + 1) * tile)
        previous = st[:, :, cols].reshape(tall, tile)
        value = jnp.concatenate([v_s[...], v_s[...]], axis=1)
        new = value + both[:tall] * (previous - value)
        st[:, :, cols] = new.reshape(rows, heads, tile)
        read = both[tall:] * new
        return read[:, :128] + read[:, 128:]

    per_part = part // tile
    for i in range(4):
        l_state[i].wait()
        for n in range(i * per_part, (i + 1) * per_part):
            r_s[...] += one_tile(n)
    r_s[...] += pltpu.roll(r_s[...], 64, 1)

    l_wg.wait()
    l_hg.wait()
    g_lin = dot(x, wg[...])
    first_head = lax.broadcasted_iota(jnp.int32, (rows, 128), 1) < 64
    gain2 = jnp.concatenate([head_gain[...], head_gain[...]], axis=1)
    for p in range(pairs):
        cols = slice(p * 128, (p + 1) * 128)
        even_head = r_s[pl.ds(2 * p, rows, heads), :]
        odd_head = r_s[pl.ds(2 * p + 1, rows, heads), :]
        even_head = even_head * lax.rsqrt(
            jnp.sum(even_head * even_head, -1, keepdims=True) / 128.0 + 1e-6
        )
        odd_head = odd_head * lax.rsqrt(
            jnp.sum(odd_head * odd_head, -1, keepdims=True) / 128.0 + 1e-6
        )
        normed = jnp.where(first_head, even_head, odd_head) * gain2
        mix[:, cols] = (normed * silu(g_lin[:, cols])).astype(BF)
    l_wo.wait()
    own_part[...] = dot(mix[...], wo[...]).astype(BF)

    pl.semaphore_wait(barrier, slots + core)

    def to_partner(src, dst, i):
        return pltpu.make_async_remote_copy(
            src_ref=src,
            dst_ref=dst,
            send_sem=tp_send.at[i],
            recv_sem=tp_recv.at[i],
            device_id=(me, 1 - core),
            device_id_type=MESH,
        )

    swap = to_partner(own_part, other_part, 0)
    swap.start()

    for load in (l_eg, l_eu, l_ed):
        load.wait()
    halves = [to_partner(eg, eg_far, 1), to_partner(eu, eu_far, 2), to_partner(ed, ed_far, 3)]
    for push in halves:
        push.start()

    for load in (l_ids, l_weight, l_mg):
        load.wait()
    small[...] = jnp.zeros_like(small)
    small[0:2, 0:rows] = ids[...].astype(F32)
    small[2:4, 0:rows] = weight[...]
    turned = small[...].T[0:rows]
    id0 = turned[:, 0:1].astype(jnp.int32)
    id1 = turned[:, 1:2].astype(jnp.int32)
    slot_iota = lax.broadcasted_iota(jnp.int32, (rows, 2 * slots), 1)
    slot_pos = lax.shift_right_logical(slot_iota, 4)
    dz = jnp.zeros_like(slot_pos)
    for pos, offset in enumerate(Z_ORDER):
        dz = jnp.where(slot_pos == pos, offset, dz)
    dy = lax.bitwise_and(lax.shift_right_logical(slot_iota, 2), 3)
    dx = lax.bitwise_and(slot_iota, 2) + core
    expert = (
        lax.bitwise_and(my_z + dz, 7) * CHIPS
        + lax.bitwise_and(my_y + dy, 3) * AXES[2]
        + lax.bitwise_and(my_x + dx, 3)
    )
    names0 = expert == id0
    names1 = expert == id1
    named = jnp.where(names0 | names1, 1.0, 0.0)
    r_iota = lax.broadcasted_iota(jnp.int32, (rows, rows), 0)
    c_iota = lax.broadcasted_iota(jnp.int32, (rows, rows), 1)
    earlier = jnp.where(c_iota < r_iota, 1.0, 0.0)
    rank = dot(earlier.astype(BF), named.astype(BF))
    slot_of = lax.bitwise_and(slot_iota, 1).astype(F32)
    takes = jnp.where(rank == slot_of, named, 0.0)
    route = jnp.where(names0, turned[:, 2:3], 0.0) + jnp.where(names1, turned[:, 3:4], 0.0)
    route = jnp.where(rank == slot_of, route, 0.0)
    route_high = route.astype(BF)
    route_low = (route - route_high.astype(F32)).astype(BF)
    route_both = jnp.concatenate([route_high.astype(F32), route_low.astype(F32)], axis=0).astype(BF)
    choose = takes.T.astype(BF)
    swap.wait()
    mixed = own_part[...].astype(F32) + other_part[...].astype(F32)
    full = x.astype(F32) + mixed
    centered = full - jnp.mean(full, -1, keepdims=True)
    variance = jnp.mean(centered * centered, -1, keepdims=True)
    after[...] = (centered * lax.rsqrt(variance + 1e-5) * mix_gain[...]).astype(BF)

    def exchange(src, dst, send_sem, recv_sem, group, sign):
        def give(slot, peer):
            pltpu.make_async_remote_copy(
                src_ref=src.at[:, slot],
                dst_ref=dst.at[:, slot],
                send_sem=send_sem,
                recv_sem=recv_sem,
                device_id=(peer, core),
                device_id_type=MESH,
            ).start()

        for pos in range(*group):
            each_of_plane(pos, sign, give)
        if group[0] <= HOME < group[1]:

            @pl.when(core == 0)
            def _():
                dst[:, SELF : SELF + 1] = src[:, SELF : SELF + 1]

    def bytes_of(src, dst, send_sem, recv_sem, first, count):
        return pltpu.make_async_remote_copy(
            src_ref=src.at[:, pl.ds(first, count)],
            dst_ref=dst.at[:, pl.ds(first, count)],
            send_sem=send_sem,
            recv_sem=recv_sem,
            device_id=(me, 1 - core),
            device_id_type=MESH,
        )

    def span(group):
        return group[0] * PLANE, group[1] * PLANE

    def arrived(src, dst, send_sem, recv_sem, group):
        first, last = span(group)
        if group[0] <= HOME < group[1]:

            @pl.when(core == 0)
            def _():
                bytes_of(src, dst, send_sem, recv_sem, first, last - first - 1).wait_recv()

            @pl.when(core == 1)
            def _():
                bytes_of(src, dst, send_sem, recv_sem, first, last - first).wait_recv()

        else:
            bytes_of(src, dst, send_sem, recv_sem, first, last - first).wait_recv()

    def put_rows(buf, values, first, last):
        for j in range(blocks):
            buf[j, first:last] = values[:, j * 128 : (j + 1) * 128].reshape(last - first, 2, 128)

    def rows_of(buf, first, last):
        return jnp.concatenate(
            [buf[j, first:last].reshape(2 * (last - first), 128) for j in range(blocks)], axis=1
        )

    for g, group in enumerate(GROUPS):
        first, last = span(group)
        put_rows(send, dot(choose[2 * first : 2 * last], after[...]).astype(BF), first, last)
        exchange(send, recv, ep_send.at[0], ep_recv.at[g], group, 1)

    l_og.wait()
    for push in halves:
        push.wait_recv()

    for g, group in enumerate(GROUPS):
        first, last = span(group)
        arrived(send, recv, ep_send.at[0], ep_recv.at[g], group)
        inputs = rows_of(recv, first, last)
        hidden = (silu(dot(inputs, eg[...])) * dot(inputs, eu[...])).astype(BF)
        hidden_far = (silu(dot(inputs, eg_far[...])) * dot(inputs, eu_far[...])).astype(BF)
        result = dot(hidden, ed[...]).astype(BF).astype(F32)
        result_far = dot(hidden_far, ed_far[...]).astype(BF).astype(F32)
        put_rows(ret_send, (result + result_far).astype(BF), first, last)
        exchange(ret_send, ret_recv, ep_send.at[1], ep_recv.at[len(GROUPS) + g], group, -1)

    moe_sum = None
    for g, group in enumerate(GROUPS):
        first, last = span(group)
        arrived(ret_send, ret_recv, ep_send.at[1], ep_recv.at[len(GROUPS) + g], group)
        both = dot(route_both[:, 2 * first : 2 * last], rows_of(ret_recv, first, last))
        both = both[:rows] + both[rows:]
        moe_sum = both if moe_sum is None else moe_sum + both
    own_moe[...] = moe_sum
    last_swap = to_partner(own_moe, other_moe, 4)
    last_swap.start()
    last_swap.wait_recv()
    final = after[...].astype(F32) + (own_moe[...] + other_moe[...])
    centered = final - jnp.mean(final, -1, keepdims=True)
    scale = lax.rsqrt(jnp.mean(centered * centered, -1, keepdims=True) + 1e-5)
    other_moe[...] = centered * scale * moe_gain[...]
    next_out[...] = other_moe[:, pl.ds(own_cols, half)].astype(BF)

    @pl.when(core == 0)
    def _():
        bytes_of(send, recv, ep_send.at[0], ep_recv.at[0], 0, slots - 1).wait_send()
        bytes_of(ret_send, ret_recv, ep_send.at[1], ep_recv.at[0], 0, slots - 1).wait_send()

    @pl.when(core == 1)
    def _():
        bytes_of(send, recv, ep_send.at[0], ep_recv.at[0], 0, slots).wait_send()
        bytes_of(ret_send, ret_recv, ep_send.at[1], ep_recv.at[0], 0, slots).wait_send()

    for remote in (*halves, last_swap):
        remote.wait_send()


def per_device(
    tokens,
    old_state,
    w_query,
    w_forget,
    w_value,
    w_gate,
    lower_bound,
    head_gain,
    w_out,
    mix_gain,
    expert_gate,
    expert_up,
    expert_down,
    expert_ids,
    route_weight,
    moe_gain,
):
    n_ep = lax.axis_size("ep")
    rows, width = tokens.shape
    heads = old_state.shape[1]
    cols = w_query.shape[1]
    units = expert_gate.shape[2]
    half = width // 2
    tall = rows * heads
    anywhere = pl.BlockSpec(memory_space=pl.ANY)
    vmem = pl.BlockSpec(memory_space=pltpu.VMEM)
    message = pltpu.VMEM((width // 128, n_ep // 2, 2, 128), BF)
    by_head = pltpu.VMEM((tall, 128), F32)
    row = pltpu.VMEM((rows, width), BF)
    return pl.pallas_call(
        kernel,
        out_shape=(
            pltpu.VMEM((rows, half), BF),
            pltpu.VMEM(old_state.shape, F32),
        ),
        in_specs=[anywhere] * 16,
        out_specs=(vmem, vmem),
        scratch_shapes=[
            row,
            *[pltpu.VMEM((width, cols), BF)] * 4,
            pltpu.VMEM((cols, width), BF),
            *[pltpu.VMEM((width, units), BF), pltpu.VMEM((width, units), BF), pltpu.VMEM((units, width), BF)] * 2,
            pltpu.VMEM((1, cols), F32),
            pltpu.VMEM((1, head_gain.shape[0]), F32),
            pltpu.VMEM((1, width), F32),
            pltpu.VMEM((2, rows), jnp.int32),
            pltpu.VMEM((2, rows), F32),
            pltpu.VMEM((1, width), F32),
            by_head,
            by_head,
            by_head,
            by_head,
            pltpu.VMEM((2 * tall, 256), BF),
            pltpu.VMEM((rows, cols), BF),
            row,
            row,
            row,
            message,
            message,
            message,
            message,
            pltpu.VMEM((rows, width), F32),
            pltpu.VMEM((rows, width), F32),
            pltpu.VMEM((8, 128), F32),
            pltpu.SemaphoreType.DMA((19,)),
            pltpu.SemaphoreType.DMA((5,)),
            pltpu.SemaphoreType.DMA((5,)),
            pltpu.SemaphoreType.DMA((2,)),
            pltpu.SemaphoreType.DMA((2 * len(GROUPS),)),
        ],
        compiler_params=pltpu.CompilerParams(
            collective_id=0, has_side_effects=True, vmem_limit_bytes=56 * 1024 * 1024
        ),
    )(
        tokens,
        old_state,
        w_query,
        w_forget,
        w_value,
        w_gate,
        lower_bound.reshape(1, cols),
        head_gain.reshape(1, -1),
        w_out,
        mix_gain.reshape(1, width),
        expert_gate,
        expert_up,
        expert_down,
        expert_ids.T,
        route_weight.T,
        moe_gain.reshape(1, width),
    )


def solution(mesh):
    in_specs = (
        P("ep", None),
        P("ep", "tp", None),
        P(None, "tp"),
        P(None, "tp"),
        P(None, "tp"),
        P(None, "tp"),
        P("tp"),
        P(),
        P("tp", None),
        P(),
        P("ep", None, "tp"),
        P("ep", None, "tp"),
        P("ep", "tp", None),
        P("ep", None),
        P("ep", None),
        P(),
    )
    out_specs = (P("ep", "tp"), P("ep", "tp", None))
    return jax.shard_map(
        per_device, mesh=mesh, in_specs=in_specs, out_specs=out_specs, check_vma=False
    )
```

time: 52 us -> 48.2 us (0.927)
  Pallas kernels: 49 us -> 45.2 us
    pallas_call x1, Pallas kernels: 49 us -> 45.2 us  [per_device(): pl.pallas_call(kernel, out_shape=(pltpu.VMEM((rows, half), BF), pltpu.VME...]
where the time goes in v3:
time: 48.2 us; the launch traced here: 48.1 us
  Pallas kernels  45.2 us (94%)
  local copies, waits for them, and re-layouts  2.29 us (5%)
  between operations  0.65 us (1%)
    pallas_call x1, Pallas kernels, per_device(): pl.pallas_call(kernel, out_shape=(pltpu.VMEM((rows, half), BF), pltpu.VME...  45.2 us
    unnamed x2, local copies, waits for them, and re-layouts  2.29 us

profile of v3, /device:TPU:1, one launch (start us, length us, event | category | flops | bytes accessed | tf_op | source)
XLA Modules:
  0.0 48.1 jit_solution(1803655199928841394)
XLA Ops:
  0.6 45.2 %shard_map.167 = (bf16[24,1024]{1,0:T(8,128)(2,1)S(1)}, f32[24,8,4096]{2,1,0:T(8,128)S(1)}) custom-call(bf16[24,2048]{1,0:T(8,128)(2,1)} %tokens.1, f32[24,8,4096]{2,1,0:T(8,128)} %old.1, bf16[2048,512]{1,0:T(8,128)(2,1)} %w_query.1, bf16[2048,512]{1,0:T(8,128)(2,1)} %w_forget.1, bf16[2048,512]{1,0:T(8,128)(2,1)} %w_value.1, bf16[2048,512]{1,0:T(8,128)(2,1)} %w_gate.1, ...), custom_call_target="tpu_custom_call" | custom-call | tf_op jit(solution)/shard_map/pallas_call | solution.py:450
  45.9 0.6 %copy.20 = bf16[24,1024]{1,0:T(8,128)(2,1)} copy(bf16[24,1024]{1,0:T(8,128)(2,1)S(1)} %get-tuple-element.2) | data formatting | bytes 98304
  46.5 1.7 %copy.21 = f32[24,8,4096]{2,1,0:T(8,128)} copy(f32[24,8,4096]{2,1,0:T(8,128)S(1)} %get-tuple-element.3) | data formatting | bytes 6291456

commit v4 on v3

--- a/solution.py
+++ b/solution.py
@@ -21,10 +21,13 @@
 AXES = (8, 4, 4)
 CHIPS = AXES[1] * AXES[2]
 PLANE = CHIPS // 2
-Z_ORDER = (3, 5, 2, 6, 4, 1, 7, 0)
-GROUPS = ((0, 2), (2, 4), (4, 5), (5, 8))
+FAR = ((4,),)
+Z_ORDER = (3, 5, 2, 6, 1, 7, 0)
+GROUPS = ((0, 2), (2, 4), (4, 7))
 HOME = Z_ORDER.index(0)
 SELF = HOME * PLANE
+RING = AXES[2]
+WIDE = 4
 
 
 def kernel(
@@ -43,8 +46,7 @@
     e_down,
     ids_in,
     weight_in,
-    moe_gain_in,
-    next_out,
+    total_out,
     st,
     tok,
     wq,
@@ -63,7 +65,6 @@
     mix_gain,
     ids,
     weight,
-    moe_gain,
     f_s,
     q_s,
     v_s,
@@ -77,6 +78,7 @@
     recv,
     ret_send,
     ret_recv,
+    far_refs,
     own_moe,
     other_moe,
     small,
@@ -85,15 +87,15 @@
     tp_recv,
     ep_send,
     ep_recv,
+    far_send_sem,
+    far_recv_sem,
 ):
     me = lax.axis_index("ep")
     core = lax.axis_index("tp")
     rows, width = tok.shape
     heads = st.shape[1]
-    half = width // 2
     blocks = width // 128
-    own_cols = pl.multiple_of(core * half, 128)
-    slots = AXES[0] * PLANE
+    slots = len(Z_ORDER) * PLANE
     n_keys = st.shape[2]
     my_z = lax.div(me, CHIPS)
     my_y = lax.rem(lax.div(me, AXES[2]), AXES[1])
@@ -104,6 +106,15 @@
         for sign in (1, -1)
         for q in (0, 1)
     }
+
+    def far_peers(g, sign):
+        for i, dz in enumerate(FAR[g]):
+            for h in range(2):
+                y = lax.rem(my_y + AXES[1] + sign * (2 * h + core), AXES[1])
+                yield 2 * i + h, z_at[(sign * dz) % AXES[0]] + y * AXES[2] + my_x
+
+    def ring_peer(dx):
+        return me - my_x + lax.rem(my_x + AXES[2] + dx, AXES[2])
 
     def each_of_plane(pos, sign, visit):
         dz = Z_ORDER[pos]
@@ -145,14 +156,13 @@
         (e_gate.at[0], eg),
         (e_up.at[0], eu),
         (e_down.at[0], ed),
-        (moe_gain_in, moe_gain),
     ]
     loads = [pltpu.make_async_copy(src, dst, in_sem.at[i]) for i, (src, dst) in enumerate(pieces)]
     for load in loads:
         load.start()
     l_tok, l_bound, l_wf, l_wq, l_wv = loads[:5]
     l_state = loads[5:9]
-    l_wg, l_hg, l_wo, l_mg, l_ids, l_weight, l_eg, l_eu, l_ed, l_og = loads[9:]
+    l_wg, l_hg, l_wo, l_mg, l_ids, l_weight, l_eg, l_eu, l_ed = loads[9:]
 
     barrier = pltpu.get_barrier_semaphore()
     pl.semaphore_signal(barrier, inc=1, device_id=(me, 1 - core), device_id_type=MESH)
@@ -160,8 +170,13 @@
     def greet(slot, peer):
         pl.semaphore_signal(barrier, inc=1, device_id=(peer, core), device_id_type=MESH)
 
-    for dz in (4, 3, 5, 2, 6, 1, 7, 0):
-        each_of_plane(Z_ORDER.index(dz), 1, greet)
+    for g in range(len(FAR)):
+        for slot, peer in far_peers(g, 1):
+            greet(slot, peer)
+    for pos in range(len(Z_ORDER)):
+        each_of_plane(pos, 1, greet)
+    for dx in range(1, RING):
+        greet(dx, ring_peer(dx))
 
     pairs = heads // 2
     tall = rows * heads
@@ -247,7 +262,8 @@
     l_wo.wait()
     own_part[...] = dot(mix[...], wo[...]).astype(BF)
 
-    pl.semaphore_wait(barrier, slots + core)
+    n_far = sum(2 * len(group) for group in FAR)
+    pl.semaphore_wait(barrier, slots + core + n_far + RING - 1)
 
     def to_partner(src, dst, i):
         return pltpu.make_async_remote_copy(
@@ -276,7 +292,7 @@
     turned = small[...].T[0:rows]
     id0 = turned[:, 0:1].astype(jnp.int32)
     id1 = turned[:, 1:2].astype(jnp.int32)
-    slot_iota = lax.broadcasted_iota(jnp.int32, (rows, 2 * slots), 1)
+    slot_iota = lax.broadcasted_iota(jnp.int32, (rows, 128), 1)
     slot_pos = lax.shift_right_logical(slot_iota, 4)
     dz = jnp.zeros_like(slot_pos)
     for pos, offset in enumerate(Z_ORDER):
@@ -303,6 +319,30 @@
     route_low = (route - route_high.astype(F32)).astype(BF)
     route_both = jnp.concatenate([route_high.astype(F32), route_low.astype(F32)], axis=0).astype(BF)
     choose = takes.T.astype(BF)
+
+    ring_of = lax.shift_right_logical(id0, 2)
+    far_takes = []
+    for group in FAR:
+        far_pos = lax.shift_right_logical(slot_iota, 3)
+        dz = jnp.zeros_like(far_pos)
+        for i, offset in enumerate(group):
+            dz = jnp.where(far_pos == i, offset, dz)
+        dy = lax.bitwise_and(lax.shift_right_logical(slot_iota, 1), 2) + core
+        ring = lax.bitwise_and(my_z + dz, 7) * AXES[1] + lax.bitwise_and(my_y + dy, 3)
+        named = jnp.where(ring == ring_of, 1.0, 0.0)
+        rank = dot(earlier.astype(BF), named.astype(BF))
+        named = jnp.where(rank == lax.bitwise_and(slot_iota, 3).astype(F32), named, 0.0)
+        far_takes.append(named)
+    far_choose = [named.T.astype(BF) for named in far_takes]
+    x_of = lax.bitwise_and(slot_iota, 3)
+    ring_weight = jnp.where(x_of == lax.bitwise_and(id0, 3), turned[:, 2:3], 0.0) + jnp.where(
+        x_of == lax.bitwise_and(id1, 3), turned[:, 3:4], 0.0
+    )
+    weight_high = ring_weight.astype(BF)
+    weight_low = (ring_weight - weight_high.astype(F32)).astype(BF)
+    weight_terms = jnp.where(
+        slot_iota < 4, weight_high.astype(F32), jnp.where(slot_iota < 8, weight_low.astype(F32), 0.0)
+    ).astype(BF)
     swap.wait()
     mixed = own_part[...].astype(F32) + other_part[...].astype(F32)
     full = x.astype(F32) + mixed
@@ -366,25 +406,94 @@
             [buf[j, first:last].reshape(2 * (last - first), 128) for j in range(blocks)], axis=1
         )
 
+    def expert(inputs):
+        hidden = (silu(dot(inputs, eg[...])) * dot(inputs, eu[...])).astype(BF)
+        hidden_far = (silu(dot(inputs, eg_far[...])) * dot(inputs, eu_far[...])).astype(BF)
+        result = dot(hidden, ed[...]).astype(BF).astype(F32)
+        result_far = dot(hidden_far, ed_far[...]).astype(BF).astype(F32)
+        return (result + result_far).astype(BF)
+
+    def far_copy(src, dst, kind, g, peer):
+        at = kind * len(FAR) + g
+        return pltpu.make_async_remote_copy(
+            src_ref=src,
+            dst_ref=dst,
+            send_sem=far_send_sem.at[at],
+            recv_sem=far_recv_sem.at[at],
+            device_id=(peer, core),
+            device_id_type=MESH,
+        )
+
+    def far_dispatch(g):
+        out, arrive = far_refs[g][0:2]
+        n = out.shape[1]
+        picked = dot(far_choose[g][: WIDE * n], after[...]).astype(BF)
+        for j in range(blocks):
+            out[j] = picked[:, j * 128 : (j + 1) * 128].reshape(n, WIDE, 128)
+        out[blocks] = dot(far_choose[g][: WIDE * n], weight_terms).astype(BF).reshape(n, WIDE, 128)
+        for slot, peer in far_peers(g, 1):
+            far_copy(out.at[:, slot], arrive.at[:, slot], 0, g, peer).start()
+
+    def far_hand_round(g):
+        out, arrive, ring_in = far_refs[g][0:3]
+        far_copy(out, arrive, 0, g, ring_peer(1)).wait_recv()
+        for dx in range(1, RING):
+            far_copy(arrive, ring_in.at[:, dx], 1, g, ring_peer(dx)).start()
+        ring_in[:, 0] = arrive[...]
+
+    def far_expert(g):
+        ring_in, back, back_in = far_refs[g][2:5]
+        n = ring_in.shape[2]
+        count = RING * n * WIDE
+        rest = pl.ds(1, RING - 1)
+        far_copy(ring_in.at[:, rest], ring_in.at[:, rest], 1, g, ring_peer(1)).wait_recv()
+        inputs = jnp.concatenate(
+            [ring_in[j].reshape(count, 128) for j in range(blocks)], axis=1
+        )
+        terms = ring_in[blocks].reshape(count, 128).astype(F32)
+        at = lax.broadcasted_iota(jnp.int32, (count, 128), 1)
+        mine = lax.bitwise_and(at, 3) == my_x
+        scale = jnp.sum(jnp.where(mine, terms, 0.0), -1, keepdims=True)
+        given = (expert(inputs).astype(F32) * scale).astype(BF)
+        for j in range(blocks):
+            back[j] = given[:, j * 128 : (j + 1) * 128].reshape(RING, n, WIDE, 128)
+        for dx in range(1, RING):
+            far_copy(back.at[:, dx], back_in.at[:, dx], 2, g, ring_peer(-dx)).start()
+        back_in[:, 0] = back[:, 0]
+
+    def far_sum(g):
+        back_in, out, home = far_refs[g][4:7]
+        n = out.shape[1]
+        rest = pl.ds(1, RING - 1)
+        far_copy(back_in.at[:, rest], back_in.at[:, rest], 2, g, ring_peer(1)).wait_recv()
+        for j in range(blocks):
+            parts = back_in[j].reshape(RING * n * WIDE, 128).astype(F32).reshape(RING, n * WIDE, 128)
+            out[j] = jnp.sum(parts, axis=0).astype(BF).reshape(n, WIDE, 128)
+        for slot, peer in far_peers(g, -1):
+            far_copy(out.at[:, slot], home.at[:, slot], 3, g, peer).start()
+
+    for g in range(len(FAR)):
+        far_dispatch(g)
     for g, group in enumerate(GROUPS):
         first, last = span(group)
         put_rows(send, dot(choose[2 * first : 2 * last], after[...]).astype(BF), first, last)
         exchange(send, recv, ep_send.at[0], ep_recv.at[g], group, 1)
 
-    l_og.wait()
+    def near_expert(g):
+        group = GROUPS[g]
+        first, last = span(group)
+        arrived(send, recv, ep_send.at[0], ep_recv.at[g], group)
+        put_rows(ret_send, expert(rows_of(recv, first, last)), first, last)
+        exchange(ret_send, ret_recv, ep_send.at[1], ep_recv.at[len(GROUPS) + g], group, -1)
+
+    far_hand_round(0)
     for push in halves:
         push.wait_recv()
-
-    for g, group in enumerate(GROUPS):
-        first, last = span(group)
-        arrived(send, recv, ep_send.at[0], ep_recv.at[g], group)
-        inputs = rows_of(recv, first, last)
-        hidden = (silu(dot(inputs, eg[...])) * dot(inputs, eu[...])).astype(BF)
-        hidden_far = (silu(dot(inputs, eg_far[...])) * dot(inputs, eu_far[...])).astype(BF)
-        result = dot(hidden, ed[...]).astype(BF).astype(F32)
-        result_far = dot(hidden_far, ed_far[...]).astype(BF).astype(F32)
-        put_rows(ret_send, (result + result_far).astype(BF), first, last)
-        exchange(ret_send, ret_recv, ep_send.at[1], ep_recv.at[len(GROUPS) + g], group, -1)
+    near_expert(0)
+    far_expert(0)
+    near_expert(1)
+    far_sum(0)
+    near_expert(2)
 
     moe_sum = None
     for g, group in enumerate(GROUPS):
@@ -393,15 +502,19 @@
         both = dot(route_both[:, 2 * first : 2 * last], rows_of(ret_recv, first, last))
         both = both[:rows] + both[rows:]
         moe_sum = both if moe_sum is None else moe_sum + both
+    for g in range(len(FAR)):
+        out, home = far_refs[g][5:7]
+        n = home.shape[1]
+        far_copy(out, home, 3, g, ring_peer(1)).wait_recv()
+        rows_back = jnp.concatenate(
+            [home[j].reshape(n * WIDE, 128) for j in range(blocks)], axis=1
+        )
+        moe_sum = moe_sum + dot(far_takes[g][:, : n * WIDE].astype(BF), rows_back)
     own_moe[...] = moe_sum
     last_swap = to_partner(own_moe, other_moe, 4)
     last_swap.start()
     last_swap.wait_recv()
-    final = after[...].astype(F32) + (own_moe[...] + other_moe[...])
-    centered = final - jnp.mean(final, -1, keepdims=True)
-    scale = lax.rsqrt(jnp.mean(centered * centered, -1, keepdims=True) + 1e-5)
-    other_moe[...] = centered * scale * moe_gain[...]
-    next_out[...] = other_moe[:, pl.ds(own_cols, half)].astype(BF)
+    total_out[...] = after[...].astype(F32) + (own_moe[...] + other_moe[...])
 
     @pl.when(core == 0)
     def _():
@@ -413,8 +526,42 @@
         bytes_of(send, recv, ep_send.at[0], ep_recv.at[0], 0, slots).wait_send()
         bytes_of(ret_send, ret_recv, ep_send.at[1], ep_recv.at[0], 0, slots).wait_send()
 
+    for g in range(len(FAR)):
+        out, arrive, ring_in, back, back_in, total, home = far_refs[g]
+        rest = pl.ds(1, RING - 1)
+        far_copy(out, arrive, 0, g, ring_peer(1)).wait_send()
+        far_copy(ring_in.at[:, rest], ring_in.at[:, rest], 1, g, ring_peer(1)).wait_send()
+        far_copy(back.at[:, rest], back_in.at[:, rest], 2, g, ring_peer(1)).wait_send()
+        far_copy(total, home, 3, g, ring_peer(1)).wait_send()
     for remote in (*halves, last_swap):
         remote.wait_send()
+
+
+def finish(total, state_in, moe_gain_in, next_out, state_out, moe_gain, normed, result, sem):
+    core = lax.axis_index("tp")
+    half = next_out.shape[1]
+    parts = sem.shape[0] - 2
+    rows = state_in.shape[0] // parts
+    gain_load = pltpu.make_async_copy(moe_gain_in, moe_gain, sem.at[parts])
+    gain_load.start()
+    copies = [
+        pltpu.make_async_copy(
+            state_in.at[pl.ds(i * rows, rows)], state_out.at[pl.ds(i * rows, rows)], sem.at[i]
+        )
+        for i in range(parts)
+    ]
+    for copy in copies:
+        copy.start()
+    values = total[...]
+    centered = values - jnp.mean(values, -1, keepdims=True)
+    scale = lax.rsqrt(jnp.mean(centered * centered, -1, keepdims=True) + 1e-5)
+    gain_load.wait()
+    normed[...] = centered * scale * moe_gain[...]
+    result[...] = normed[:, pl.ds(pl.multiple_of(core * half, 128), half)].astype(BF)
+    copies.append(pltpu.make_async_copy(result, next_out, sem.at[parts + 1]))
+    copies[-1].start()
+    for copy in copies:
+        copy.wait()
 
 
 def per_device(
@@ -435,7 +582,6 @@
     route_weight,
     moe_gain,
 ):
-    n_ep = lax.axis_size("ep")
     rows, width = tokens.shape
     heads = old_state.shape[1]
     cols = w_query.shape[1]
@@ -444,16 +590,29 @@
     tall = rows * heads
     anywhere = pl.BlockSpec(memory_space=pl.ANY)
     vmem = pl.BlockSpec(memory_space=pltpu.VMEM)
-    message = pltpu.VMEM((width // 128, n_ep // 2, 2, 128), BF)
+    blocks = width // 128
+    message = pltpu.VMEM((blocks, len(Z_ORDER) * PLANE, 2, 128), BF)
+    far = tuple(
+        (
+            pltpu.VMEM((blocks + 1, 2 * len(group), WIDE, 128), BF),
+            pltpu.VMEM((blocks + 1, 2 * len(group), WIDE, 128), BF),
+            pltpu.VMEM((blocks + 1, RING, 2 * len(group), WIDE, 128), BF),
+            pltpu.VMEM((blocks, RING, 2 * len(group), WIDE, 128), BF),
+            pltpu.VMEM((blocks, RING, 2 * len(group), WIDE, 128), BF),
+            pltpu.VMEM((blocks, 2 * len(group), WIDE, 128), BF),
+            pltpu.VMEM((blocks, 2 * len(group), WIDE, 128), BF),
+        )
+        for group in FAR
+    )
     by_head = pltpu.VMEM((tall, 128), F32)
     row = pltpu.VMEM((rows, width), BF)
-    return pl.pallas_call(
+    total, new_state = pl.pallas_call(
         kernel,
         out_shape=(
-            pltpu.VMEM((rows, half), BF),
+            pltpu.VMEM((rows, width), F32),
             pltpu.VMEM(old_state.shape, F32),
         ),
-        in_specs=[anywhere] * 16,
+        in_specs=[anywhere] * 15,
         out_specs=(vmem, vmem),
         scratch_shapes=[
             row,
@@ -465,7 +624,6 @@
             pltpu.VMEM((1, width), F32),
             pltpu.VMEM((2, rows), jnp.int32),
             pltpu.VMEM((2, rows), F32),
-            pltpu.VMEM((1, width), F32),
             by_head,
             by_head,
             by_head,
@@ -479,14 +637,17 @@
             message,
             message,
             message,
+            far,
             pltpu.VMEM((rows, width), F32),
             pltpu.VMEM((rows, width), F32),
             pltpu.VMEM((8, 128), F32),
-            pltpu.SemaphoreType.DMA((19,)),
+            pltpu.SemaphoreType.DMA((18,)),
             pltpu.SemaphoreType.DMA((5,)),
             pltpu.SemaphoreType.DMA((5,)),
             pltpu.SemaphoreType.DMA((2,)),
             pltpu.SemaphoreType.DMA((2 * len(GROUPS),)),
+            pltpu.SemaphoreType.DMA((4 * len(FAR),)),
+            pltpu.SemaphoreType.DMA((4 * len(FAR),)),
         ],
         compiler_params=pltpu.CompilerParams(
             collective_id=0, has_side_effects=True, vmem_limit_bytes=56 * 1024 * 1024
@@ -507,6 +668,24 @@
         expert_down,
         expert_ids.T,
         route_weight.T,
+    )
+    return pl.pallas_call(
+        finish,
+        out_shape=(
+            jax.ShapeDtypeStruct((rows, half), BF),
+            jax.ShapeDtypeStruct(old_state.shape, F32),
+        ),
+        in_specs=[vmem, vmem, anywhere],
+        out_specs=(anywhere, anywhere),
+        scratch_shapes=[
+            pltpu.VMEM((1, width), F32),
+            pltpu.VMEM((rows, width), F32),
+            pltpu.VMEM((rows, half), BF),
+            pltpu.SemaphoreType.DMA((6,)),
+        ],
+    )(
+        pltpu.with_memory_space_constraint(total, pltpu.VMEM),
+        pltpu.with_memory_space_constraint(new_state, pltpu.VMEM),
         moe_gain.reshape(1, width),
     )
 

time: 48.2 us -> 46.2 us (0.959)
  local copies, waits for them, and re-layouts: 2.29 us -> 0 us
    unnamed x2 -> x0, local copies, waits for them, and re-layouts: 2.29 us -> none
    pallas_call x1 -> x2, Pallas kernels: 45.2 us -> 45.4 us  [the longest x1 43.7 us: per_device(): pl.pallas_call(kernel, out_shape=(pltpu.VMEM((rows, width), F32), pltpu.V...]
where the time goes in v4:
time: 46.2 us; the launch traced here: 46 us
  Pallas kernels  45.4 us (98%)
  between operations  0.64 us (1%)
    pallas_call x1, Pallas kernels, per_device(): pl.pallas_call(kernel, out_shape=(pltpu.VMEM((rows, width), F32), pltpu.V...  43.7 us
    pallas_call x1, Pallas kernels, per_device(): pl.pallas_call(finish, out_shape=(jax.ShapeDtypeStruct((rows, half), BF),...  1.71 us

profile of v4, /device:TPU:1, one launch (start us, length us, event | category | flops | bytes accessed | tf_op | source)
XLA Modules:
  0.0 46.0 jit_solution(6477716210147135697)
XLA Ops:
  0.6 43.7 %shard_map.167 = (f32[24,2048]{1,0:T(8,128)S(1)}, f32[24,8,4096]{2,1,0:T(8,128)S(1)}) custom-call(bf16[24,2048]{1,0:T(8,128)(2,1)} %tokens.1, f32[24,8,4096]{2,1,0:T(8,128)} %old.1, bf16[2048,512]{1,0:T(8,128)(2,1)} %w_query.1, bf16[2048,512]{1,0:T(8,128)(2,1)} %w_forget.1, bf16[2048,512]{1,0:T(8,128)(2,1)} %w_value.1, bf16[2048,512]{1,0:T(8,128)(2,1)} %w_gate.1, ...), custom_call_target="tpu_custom_call" | custom-call | tf_op jit(solution)/shard_map/pallas_call | solution.py:609
  44.3 1.7 %shard_map.168 = (bf16[24,1024]{1,0:T(8,128)(2,1)}, f32[24,8,4096]{2,1,0:T(8,128)}) custom-call(f32[24,2048]{1,0:T(8,128)S(1)} %get-tuple-element.4.total, f32[24,8,4096]{2,1,0:T(8,128)S(1)} %get-tuple-element.5.state_in, f32[1,2048]{1,0:T(1,128)} %bitcast.7), custom_call_target="tpu_custom_call" | custom-call | tf_op jit(solution)/shard_map/pallas_call | solution.py:672

commit v5 on v4

--- a/solution.py
+++ b/solution.py
@@ -474,10 +474,10 @@
 
     for g in range(len(FAR)):
         far_dispatch(g)
-    for g, group in enumerate(GROUPS):
-        first, last = span(group)
+    def near_dispatch(g):
+        first, last = span(GROUPS[g])
         put_rows(send, dot(choose[2 * first : 2 * last], after[...]).astype(BF), first, last)
-        exchange(send, recv, ep_send.at[0], ep_recv.at[g], group, 1)
+        exchange(send, recv, ep_send.at[0], ep_recv.at[g], GROUPS[g], 1)
 
     def near_expert(g):
         group = GROUPS[g]
@@ -486,7 +486,10 @@
         put_rows(ret_send, expert(rows_of(recv, first, last)), first, last)
         exchange(ret_send, ret_recv, ep_send.at[1], ep_recv.at[len(GROUPS) + g], group, -1)
 
+    near_dispatch(0)
     far_hand_round(0)
+    near_dispatch(1)
+    near_dispatch(2)
     for push in halves:
         push.wait_recv()
     near_expert(0)
@@ -513,9 +516,6 @@
     own_moe[...] = moe_sum
     last_swap = to_partner(own_moe, other_moe, 4)
     last_swap.start()
-    last_swap.wait_recv()
-    total_out[...] = after[...].astype(F32) + (own_moe[...] + other_moe[...])
-
     @pl.when(core == 0)
     def _():
         bytes_of(send, recv, ep_send.at[0], ep_recv.at[0], 0, slots - 1).wait_send()
@@ -533,8 +533,11 @@
         far_copy(ring_in.at[:, rest], ring_in.at[:, rest], 1, g, ring_peer(1)).wait_send()
         far_copy(back.at[:, rest], back_in.at[:, rest], 2, g, ring_peer(1)).wait_send()
         far_copy(total, home, 3, g, ring_peer(1)).wait_send()
-    for remote in (*halves, last_swap):
+    for remote in halves:
         remote.wait_send()
+    last_swap.wait_recv()
+    total_out[...] = after[...].astype(F32) + (own_moe[...] + other_moe[...])
+    last_swap.wait_send()
 
 
 def finish(total, state_in, moe_gain_in, next_out, state_out, moe_gain, normed, result, sem):

time: 46.2 us -> 45.7 us (0.989)
  Pallas kernels: 45.4 us -> 44.9 us
    pallas_call x1, Pallas kernels: 43.7 us -> 43.2 us  [per_device(): pl.pallas_call(kernel, out_shape=(pltpu.VMEM((rows, width), F32), pltpu.V...]
where the time goes in v5:
time: 45.7 us; the launch traced here: 45.6 us
  Pallas kernels  44.9 us (98%)
  between operations  0.64 us (1%)
    pallas_call x1, Pallas kernels, per_device(): pl.pallas_call(kernel, out_shape=(pltpu.VMEM((rows, width), F32), pltpu.V...  43.2 us
    pallas_call x1, Pallas kernels, per_device(): pl.pallas_call(finish, out_shape=(jax.ShapeDtypeStruct((rows, half), BF),...  1.71 us

profile of v5, /device:TPU:1, one launch (start us, length us, event | category | flops | bytes accessed | tf_op | source)
XLA Modules:
  0.0 45.6 jit_solution(2982480567501850187)
XLA Ops:
  0.6 43.2 %shard_map.167 = (f32[24,2048]{1,0:T(8,128)S(1)}, f32[24,8,4096]{2,1,0:T(8,128)S(1)}) custom-call(bf16[24,2048]{1,0:T(8,128)(2,1)} %tokens.1, f32[24,8,4096]{2,1,0:T(8,128)} %old.1, bf16[2048,512]{1,0:T(8,128)(2,1)} %w_query.1, bf16[2048,512]{1,0:T(8,128)(2,1)} %w_forget.1, bf16[2048,512]{1,0:T(8,128)(2,1)} %w_value.1, bf16[2048,512]{1,0:T(8,128)(2,1)} %w_gate.1, ...), custom_call_target="tpu_custom_call" | custom-call | tf_op jit(solution)/shard_map/pallas_call | solution.py:612
  43.8 1.7 %shard_map.168 = (bf16[24,1024]{1,0:T(8,128)(2,1)}, f32[24,8,4096]{2,1,0:T(8,128)}) custom-call(f32[24,2048]{1,0:T(8,128)S(1)} %get-tuple-element.4.total, f32[24,8,4096]{2,1,0:T(8,128)S(1)} %get-tuple-element.5.state_in, f32[1,2048]{1,0:T(1,128)} %bitcast.7), custom_call_target="tpu_custom_call" | custom-call | tf_op jit(solution)/shard_map/pallas_call | solution.py:675

commit v6 on v5

--- a/solution.py
+++ b/solution.py
@@ -513,9 +513,10 @@
             [home[j].reshape(n * WIDE, 128) for j in range(blocks)], axis=1
         )
         moe_sum = moe_sum + dot(far_takes[g][:, : n * WIDE].astype(BF), rows_back)
-    own_moe[...] = moe_sum
+    own_moe[...] = moe_sum.astype(BF)
     last_swap = to_partner(own_moe, other_moe, 4)
     last_swap.start()
+    total_out[...] = after[...].astype(F32) + moe_sum
     @pl.when(core == 0)
     def _():
         bytes_of(send, recv, ep_send.at[0], ep_recv.at[0], 0, slots - 1).wait_send()
@@ -536,7 +537,7 @@
     for remote in halves:
         remote.wait_send()
     last_swap.wait_recv()
-    total_out[...] = after[...].astype(F32) + (own_moe[...] + other_moe[...])
+    total_out[...] += other_moe[...].astype(F32)
     last_swap.wait_send()
 
 
@@ -641,8 +642,8 @@
             message,
             message,
             far,
-            pltpu.VMEM((rows, width), F32),
-            pltpu.VMEM((rows, width), F32),
+            row,
+            row,
             pltpu.VMEM((8, 128), F32),
             pltpu.SemaphoreType.DMA((18,)),
             pltpu.SemaphoreType.DMA((5,)),

time: 45.7 us -> 45.6 us (level)
  no operation moved by 1% of the time
where the time goes in v6:
time: 45.6 us; the launch traced here: 45.4 us
  Pallas kernels  44.8 us (98%)
  between operations  0.64 us (1%)
    pallas_call x1, Pallas kernels, per_device(): pl.pallas_call(kernel, out_shape=(pltpu.VMEM((rows, width), F32), pltpu.V...  43 us
    pallas_call x1, Pallas kernels, per_device(): pl.pallas_call(finish, out_shape=(jax.ShapeDtypeStruct((rows, half), BF),...  1.71 us

profile of v6, /device:TPU:1, one launch (start us, length us, event | category | flops | bytes accessed | tf_op | source)
XLA Modules:
  0.0 45.4 jit_solution(15686724671775393523)
XLA Ops:
  0.6 43.0 %shard_map.167 = (f32[24,2048]{1,0:T(8,128)S(1)}, f32[24,8,4096]{2,1,0:T(8,128)S(1)}) custom-call(bf16[24,2048]{1,0:T(8,128)(2,1)} %tokens.1, f32[24,8,4096]{2,1,0:T(8,128)} %old.1, bf16[2048,512]{1,0:T(8,128)(2,1)} %w_query.1, bf16[2048,512]{1,0:T(8,128)(2,1)} %w_forget.1, bf16[2048,512]{1,0:T(8,128)(2,1)} %w_value.1, bf16[2048,512]{1,0:T(8,128)(2,1)} %w_gate.1, ...), custom_call_target="tpu_custom_call" | custom-call | tf_op jit(solution)/shard_map/pallas_call | solution.py:613
  43.7 1.7 %shard_map.168 = (bf16[24,1024]{1,0:T(8,128)(2,1)}, f32[24,8,4096]{2,1,0:T(8,128)}) custom-call(f32[24,2048]{1,0:T(8,128)S(1)} %get-tuple-element.4.total, f32[24,8,4096]{2,1,0:T(8,128)S(1)} %get-tuple-element.5.state_in, f32[1,2048]{1,0:T(1,128)} %bitcast.7), custom_call_target="tpu_custom_call" | custom-call | tf_op jit(solution)/shard_map/pallas_call | solution.py:676
